TPU v7x, 256 devices: a 4x2x16 block of a 4x16x16 slice. The times are simulated.
256 devices in a mesh: grp: 2 (over y), fs: 16 (over z), tp: 8 (over x, core).
Axes of the slice: x: 4, y: 2, z: 16, core: 2. Of those that a mesh axis runs over, the one named last changes fastest.
The devices are a block of a 4x16x16 slice.
Arguments:
- tokens: bfloat16 [32768, 2048], P(('grp', 'fs', 'tp')), parts along dimension 0, may hold values from -6 to 6
- route_ids: int32 [32768, 8], P(('grp', 'fs', 'tp')), parts along dimension 0, may hold values from 0 to 127, all different within a row; in each aligned block of 128 rows (0 to 127, 128 to 255, ...) at most 12 rows name the same one
- route_scores: float32 [32768, 8], P(('grp', 'fs', 'tp')), parts along dimension 0, may hold values from 0.05 to 1
- norm_gain: float32 [2048], P('fs'), may hold values from 0.1 to 1.9
- expert_gate: float32 [128, 2048, 256], P(None, 'fs', 'tp'), may hold values from -0.125 to 0.125
- expert_up: float32 [128, 2048, 256], P(None, 'fs', 'tp'), may hold values from -0.125 to 0.125
- expert_down: float32 [128, 256, 2048], P(None, 'fs', 'tp'), may hold values from -0.375 to 0.375
- shared_gate: float32 [2048, 256], P('fs', 'tp'), may hold values from -0.125 to 0.125
- shared_up: float32 [2048, 256], P('fs', 'tp'), may hold values from -0.125 to 0.125
- shared_down: float32 [256, 2048], P('fs', 'tp'), may hold values from -0.375 to 0.375
Outputs:
- mixed: bfloat16 [32768, 2048], P(('grp', 'fs', 'tp')), parts along dimension 0
- sampler_gate: bfloat16 [256, 2048, 256], P(('grp', 'fs', 'tp')), parts along dimension 0
- sampler_up: bfloat16 [256, 2048, 256], P(('grp', 'fs', 'tp')), parts along dimension 0
- sampler_down: bfloat16 [256, 256, 2048], P(('grp', 'fs', 'tp')), parts along dimension 0
- sampler_shared_gate: bfloat16 [4096, 256], P(('grp', 'fs')), parts along dimension 0
- sampler_shared_up: bfloat16 [4096, 256], P(('grp', 'fs')), parts along dimension 0
- sampler_shared_down: bfloat16 [512, 2048], P(('grp', 'fs')), parts along dimension 0
There are 2 independent parts, one for each index of `grp`. A program takes and returns all parts, laid end to end along the dimension named above; an argument that names none is the same for every part. Nothing has to cross between parts.
Inputs may be any that keep to these rules, and one draw needn't show every extreme that they name: `route_ids`: each row names 8 different experts. Among the 128 rows of one device no expert is named more than 12 times, a bound that some block reaches.
All inputs are finite; a program needn't handle non-finite values.
Results may differ from a plain program's by a relative error of at most 0.0084.
Values may be sent and summed in bfloat16 or wider, within the bound.
A program may use at most 128 MiB of HBM per device.

v0:
```python
import jax
import jax.numpy as jnp
from jax import lax
from jax.sharding import PartitionSpec as P

EPSILON = 1e-06
route_scale = 2.5


def in_blocks(array, dim, count):
    shape = array.shape
    tiles = array.reshape(*shape[:dim], count, shape[dim] // count, *shape[dim + 1 :])
    return jnp.moveaxis(tiles, dim, 0)


def laid_out(tiles, dim):
    tiles = jnp.moveaxis(tiles, 0, dim)
    shape = tiles.shape
    return tiles.reshape(*shape[:dim], shape[dim] * shape[dim + 1], *shape[dim + 2 :])


def joined_exchange(array, axis, axes, splits, concats):
    sizes = [lax.axis_size(a) for a in axes]
    tiles = in_blocks(array, splits[0], sizes[0])
    tiles = jnp.moveaxis(in_blocks(tiles, splits[1] + 1, sizes[1]), 0, 1)
    inside = tiles.shape[2:]
    tiles = tiles.reshape(-1, *inside)
    tiles = lax.all_to_all(tiles, axis, split_axis=0, concat_axis=0, tiled=True)
    tiles = laid_out(tiles.reshape(*sizes, *inside), concats[0] + 1)
    return laid_out(tiles, concats[1])


def side_by_side(arrays, axis, dim, along):
    ends, at = ([], 0)
    for a in arrays[:-1]:
        at += a.shape[along]
        ends.append(at)
    both = jnp.concatenate(arrays, axis=along)
    return tuple(jnp.split(lax.all_gather(both, axis, axis=dim, tiled=True), ends, axis=along))


def expert_rows(row_block, w_gate, w_up, w_down):
    gate_rows = jnp.dot(row_block, w_gate, preferred_element_type=jnp.float32)
    up_rows = jnp.dot(row_block, w_up, preferred_element_type=jnp.float32)
    hidden = (jax.nn.silu(gate_rows) * up_rows).astype(jnp.bfloat16)
    return jnp.dot(hidden, w_down, preferred_element_type=jnp.float32).astype(jnp.bfloat16)


def on_device(
    tokens,
    route_ids,
    route_scores,
    norm_gain,
    expert_gate,
    expert_up,
    expert_down,
    shared_gate,
    shared_up,
    shared_down,
):
    fs_count = lax.axis_size("fs")
    tp_count = lax.axis_size("tp")
    experts = fs_count * tp_count
    gain_col = norm_gain[:, None]
    piece_gate = (gain_col[None] * expert_gate).astype(jnp.bfloat16)
    piece_up = (gain_col[None] * expert_up).astype(jnp.bfloat16)
    piece_down = expert_down.astype(jnp.bfloat16)
    moved = (
        joined_exchange(
            piece_gate.reshape((fs_count, tp_count) + piece_gate.shape[1:]),
            ("fs", "tp"),
            ("fs", "tp"),
            (0, 1),
            (2, 3),
        ),
        joined_exchange(
            piece_up.reshape((fs_count, tp_count) + piece_up.shape[1:]),
            ("fs", "tp"),
            ("fs", "tp"),
            (0, 1),
            (2, 3),
        ),
        joined_exchange(
            piece_down.reshape((fs_count, tp_count) + piece_down.shape[1:]),
            ("fs", "tp"),
            ("fs", "tp"),
            (0, 1),
            (2, 3),
        ),
    )
    served_gate = moved[0].reshape(moved[0].shape[1:])
    served_up = moved[1].reshape(moved[1].shape[1:])
    served_down = moved[2].reshape(moved[2].shape[1:])
    tile_gate = (gain_col * shared_gate).astype(jnp.bfloat16)
    tile_up = (gain_col * shared_up).astype(jnp.bfloat16)
    tile_down = shared_down.astype(jnp.bfloat16)
    held_gate, held_up, held_down = (
        *side_by_side((tile_gate, tile_up), "tp", 1, 0),
        lax.all_gather(tile_down, "tp", axis=1, tiled=True),
    )
    rows_dev = tokens.shape[0]
    width = tokens.shape[1]
    picks = route_ids.shape[1]
    capacity = 3 * rows_dev * picks // (2 * experts)
    widened = tokens.astype(jnp.float32)
    normed = (
        widened * lax.rsqrt(jnp.mean(widened * widened, axis=1, keepdims=True) + EPSILON)
    ).astype(jnp.bfloat16)
    weights = route_scale * route_scores / jnp.sum(route_scores, axis=1, keepdims=True)
    flat_ids = route_ids.reshape(-1)
    onehot = (flat_ids[:, None] == jnp.arange(experts, dtype=jnp.int32)[None, :]).astype(jnp.int32)
    earlier = jnp.cumsum(onehot, axis=0) - onehot
    ranks = jnp.sum(earlier * onehot, axis=1)
    target = flat_ids * capacity + ranks
    outbox = (
        jnp.zeros((experts * capacity, width), jnp.bfloat16)
        .at[target]
        .set(jnp.repeat(normed, picks, axis=0))
    )
    arrived = lax.all_to_all(
        lax.all_to_all(
            outbox.reshape(fs_count, tp_count, capacity, width),
            "fs",
            split_axis=0,
            concat_axis=0,
            tiled=True,
        ),
        "tp",
        split_axis=1,
        concat_axis=1,
        tiled=True,
    )
    finished = expert_rows(
        arrived.reshape(-1, width), served_gate[0], served_up[0], served_down[0]
    ).reshape(arrived.shape)
    returned = joined_exchange(finished, ("fs", "tp"), ("fs", "tp"), (0, 1), (0, 1))
    results = returned.reshape(experts * capacity, width)[target]
    routed = jnp.sum(
        results.reshape(rows_dev, picks, width).astype(jnp.float32) * weights[:, :, None], axis=1
    )
    pieces = side_by_side((held_gate, held_up), "fs", 0, 1)
    columns = normed
    gate_part = jnp.dot(columns, pieces[0], preferred_element_type=jnp.float32)
    up_part = jnp.dot(columns, pieces[1], preferred_element_type=jnp.float32)
    shared_hidden = (jax.nn.silu(gate_part) * up_part).astype(jnp.bfloat16)
    columns = shared_hidden
    shared_term = jnp.dot(
        columns,
        lax.all_gather(held_down, "fs", axis=0, tiled=True),
        preferred_element_type=jnp.float32,
    )
    mixed = (routed + shared_term).astype(jnp.bfloat16)
    return (mixed, served_gate, served_up, served_down, held_gate, held_up, held_down)


def solution(mesh):
    return jax.shard_map(
        on_device,
        mesh=mesh,
        in_specs=(
            P(("grp", "fs", "tp"), None),
            P(("grp", "fs", "tp"), None),
            P(("grp", "fs", "tp"), None),
            P("fs"),
            P(None, "fs", "tp"),
            P(None, "fs", "tp"),
            P(None, "fs", "tp"),
            P("fs", "tp"),
            P("fs", "tp"),
            P("fs", "tp"),
        ),
        out_specs=(
            P(("grp", "fs", "tp"), None),
            P(("grp", "fs", "tp"), None, None),
            P(("grp", "fs", "tp"), None, None),
            P(("grp", "fs", "tp"), None, None),
            P(("grp", "fs"), None),
            P(("grp", "fs"), None),
            P(("grp", "fs"), None),
        ),
        check_vma=False,
    )
```

profile of v0, /device:TPU:33, one launch (start us, length us, event | category | flops | bytes accessed | tf_op | source)
XLA Modules:
  0.0 1078.0 jit_solution(16479098686624307019)
XLA Ops:
  7.2 3.7 fusion.10
  10.9 81.9 %all_to_all.30 = bf16[128,1,1,128,32]{3,4,2,1,0:T(8,128)(2,1)S(1)} all-to-all(bf16[128,1,1,128,32]{3,4,2,1,0:T(8,128)(2,1)S(1)} %get-tuple-element.39), channel_id=1, replica_groups=mesh['grp'=2,'fs'=16,'tp'=8] {'fs','tp'}, dimensions={0} | all-to-all | bytes 2097152 | tf_op jit(solution)/shard_map/all_to_all | solution.py:28
  92.8 12.3 %all-to-all-start.3 = ((bf16[128,1,1,128,32]{3,4,2,1,0:T(8,128)(2,1)}), bf16[128,1,1,128,32]{3,4,2,1,0:T(8,128)(2,1)S(1)}, u32[]{:S(2)}, u32[]{:S(2)}) async-start(bf16[128,1,1,128,32]{3,4,2,1,0:T(8,128)(2,1)} %get-tuple-element.40), calls=%async_computation.3 | async-start | bytes 2097152 | tf_op jit(solution)/shard_map/all_to_all | solution.py:28
  105.6 0.2 fusion.19
  106.2 0.4 fusion.18
  106.6 0.2 fusion.8
  106.8 0.2 fusion.9
  106.9 10.2 scatter_custom_fusion
  117.2 10.6 reshape.110
  127.8 10.7 copy.75
  138.5 17.2 %all-to-all-done.3 = bf16[128,1,1,128,32]{3,4,2,1,0:T(8,128)(2,1)S(1)} async-done(((bf16[128,1,1,128,32]{3,4,2,1,0:T(8,128)(2,1)}), bf16[128,1,1,128,32]{3,4,2,1,0:T(8,128)(2,1)S(1)}, u32[]{:S(2)}, u32[]{:S(2)}) %all-to-all-start.3) | async-done | bytes 1048608 | tf_op jit(solution)/shard_map/all_to_all | solution.py:28
  155.8 7.9 all-to-all-start
  163.7 2.7 convert_bitcast_fusion
  166.4 269.4 %all-to-all-done = bf16[16,8,12,2048]{3,1,2,0:T(8,128)(2,1)} async-done(((bf16[16,8,12,2048]{3,1,2,0:T(8,128)(2,1)}), bf16[16,8,12,2048]{3,1,2,0:T(8,128)(2,1)}, u32[]{:S(2)}, u32[]{:S(2)}) %all-to-all-start) | async-done | bytes 6291488 | tf_op jit(solution)/shard_map/all_to_all | solution.py:121
  435.8 16.5 %all-to-all-start.4 = ((bf16[128,1,1,16,256]{4,3,2,1,0:T(8,128)(2,1)}), bf16[128,1,1,16,256]{4,3,2,1,0:T(8,128)(2,1)}, u32[]{:S(2)}, u32[]{:S(2)}) async-start(bf16[128,1,1,16,256]{4,3,2,1,0:T(8,128)(2,1)} %convert_bitcast_fusion), calls=%async_computation.4 | async-start | bytes 2097152 | tf_op jit(solution)/shard_map/all_to_all | solution.py:28
  452.3 8.9 copy.76
  461.2 42.1 %all-to-all-done.4 = bf16[128,1,1,16,256]{4,3,2,1,0:T(8,128)(2,1)} async-done(((bf16[128,1,1,16,256]{4,3,2,1,0:T(8,128)(2,1)}), bf16[128,1,1,16,256]{4,3,2,1,0:T(8,128)(2,1)}, u32[]{:S(2)}, u32[]{:S(2)}) %all-to-all-start.4) | async-done | bytes 1048608 | tf_op jit(solution)/shard_map/all_to_all | solution.py:28
  503.3 7.4 all-to-all-start.1
  510.7 1.6 copy.94
  512.4 1.5 reshape.113
  513.9 1.6 copy.93
  515.5 1.5 reshape.115
  517.1 2.3 copy.81
  519.4 2.3 copy.82
  521.6 60.4 %all-to-all-done.1 = bf16[16,8,12,2048]{3,0,2,1:T(8,128)(2,1)} async-done(((bf16[16,8,12,2048]{3,0,2,1:T(8,128)(2,1)}), bf16[16,8,12,2048]{3,0,2,1:T(8,128)(2,1)}, u32[]{:S(2)}, u32[]{:S(2)}) %all-to-all-start.1) | async-done | bytes 6291488 | tf_op jit(solution)/shard_map/all_to_all | solution.py:120
  582.1 9.7 copy.77
  591.7 10.8 %reshape.111 = bf16[1536,2048]{1,0:T(8,128)(2,1)} reshape(bf16[16,8,12,2048]{3,2,1,0:T(8,128)(2,1)} %copy.77) | data formatting | bytes 12582912 | tf_op jit(solution)/shard_map/reshape | solution.py:134
  602.6 5.8 fusion.31
  608.3 12.6 %convolution_convert_fusion = bf16[1536,2048]{1,0:T(8,128)(2,1)} fusion(bf16[256,2048]{0,1:T(8,128)(2,1)} %bitcast.85, bf16[1536,2048]{1,0:T(8,128)(2,1)} %reshape.111, bf16[2048,256]{0,1:T(8,128)(2,1)S(1)} %bitcast.82, f32[1536,256]{1,0:T(8,128)} %fusion.31), kind=kOutput, calls=%fused_computation.4 | convolution fusion | flops 3226730496 | bytes 16252928 | tf_op jit(solution)/shard_map/dot_general | solution.py:46
  620.9 10.6 reshape_transpose_transpose_reshape_reshape_reshape.15
  631.6 10.2 all-to-all-start.5
  641.9 16.9 %all_gather.12 = bf16[256,256]{0,1:T(8,128)(2,1)S(1)} all-gather(bf16[256,32]{0,1:T(8,128)(2,1)S(1)} %pad_maximum_fusion.1), channel_id=1, replica_groups=mesh['grp'=2,'fs'=16,'tp'=8] {'tp'}, dimensions={1}, use_global_device_ids=true | all-gather | bytes 147456 | tf_op jit(solution)/shard_map/all_gather | solution.py:39
  658.8 0.7 pad_maximum_fusion
  659.6 14.0 %all_gather.14 = bf16[16,2048]{1,0:T(8,128)(2,1)} all-gather(bf16[16,256]{1,0:T(8,128)(2,1)S(1)} %convert_element_type.63), channel_id=1, replica_groups=mesh['grp'=2,'fs'=16,'tp'=8] {'tp'}, dimensions={1}, use_global_device_ids=true | all-gather | bytes 73728 | tf_op jit(solution)/shard_map/all_gather | solution.py:99
  673.7 0.7 copy.89
  674.5 0.7 copy.90
  675.2 0.1 copy.84
  675.3 173.9 %all-gather.3.cloned.1.call-done = bf16[2048,512]{0,1:T(8,128)(2,1)} async-done(((bf16[128,512]{0,1:T(8,128)(2,1)}), bf16[2048,512]{0,1:T(8,128)(2,1)}) %all-gather.3.cloned.1.call-update) | async-done | bytes 2097168 | tf_op jit(solution)/shard_map/all_gather | solution.py:39
  849.2 1.7 fusion.14
  851.0 1.3 copy.86
  852.3 1.3 copy.87
  853.6 2.3 copy.88
  855.8 181.6 %all-to-all-done.5 = bf16[128,1,1,12,2048]{4,3,2,1,0:T(8,128)(2,1)} async-done(((bf16[128,1,1,12,2048]{4,3,2,1,0:T(8,128)(2,1)}), bf16[128,1,1,12,2048]{4,3,2,1,0:T(8,128)(2,1)}, u32[]{:S(2)}, u32[]{:S(2)}) %all-to-all-start.5) | async-done | bytes 6291488 | tf_op jit(solution)/shard_map/all_to_all | solution.py:28
  1037.4 10.7 reshape_reshape.12
  1048.1 12.4 %gather_fusion = bf16[1024,2048]{1,0:T(8,128)(2,1)} fusion(bf16[1536,2048]{1,0:T(8,128)(2,1)} %reshape_reshape.12, s32[1024]{0:T(1024)S(1)} %broadcast_clamp_fusion), kind=kCustom, calls=%fused_computation | custom fusion | bytes 8392704 | tf_op jit(solution)/shard_map/gather | solution.py:137
  1060.5 6.5 fusion
  1067.0 3.3 fusion.5
  1070.3 0.6 copy.96
  (42 shorter events, 1.1 us)
Async XLA Ops:
  7.2 98.0 %copy-start.4 = (s32[128,8]{0,1:T(8,128)S(1)}, s32[128,8]{0,1:T(8,128)}, u32[]{:S(2)}) copy-start(s32[128,8]{0,1:T(8,128)} %param.11) | copy-start | bytes 12292
  10.9 95.6 %copy-start = (bf16[128,2048]{1,0:T(8,128)(2,1)S(1)}, bf16[128,2048]{1,0:T(8,128)(2,1)}, u32[]{:S(2)}) copy-start(bf16[128,2048]{1,0:T(8,128)(2,1)} %param.10) | copy-start | bytes 1572868
  92.8 62.9 %all-to-all-start.3 = ((bf16[128,1,1,128,32]{3,4,2,1,0:T(8,128)(2,1)}), bf16[128,1,1,128,32]{3,4,2,1,0:T(8,128)(2,1)S(1)}, u32[]{:S(2)}, u32[]{:S(2)}) async-start(bf16[128,1,1,128,32]{3,4,2,1,0:T(8,128)(2,1)} %get-tuple-element.40), calls=%async_computation.3 | async-start | bytes 2097152 | tf_op jit(solution)/shard_map/all_to_all | solution.py:28
  155.8 280.0 %all-to-all-start = ((bf16[16,8,12,2048]{3,1,2,0:T(8,128)(2,1)}), bf16[16,8,12,2048]{3,1,2,0:T(8,128)(2,1)}, u32[]{:S(2)}, u32[]{:S(2)}) async-start(bf16[16,8,12,2048]{3,1,2,0:T(8,128)(2,1)} %copy.75), calls=%async_computation | async-start | bytes 12582912 | tf_op jit(solution)/shard_map/all_to_all | solution.py:121
  435.8 67.5 %all-to-all-start.4 = ((bf16[128,1,1,16,256]{4,3,2,1,0:T(8,128)(2,1)}), bf16[128,1,1,16,256]{4,3,2,1,0:T(8,128)(2,1)}, u32[]{:S(2)}, u32[]{:S(2)}) async-start(bf16[128,1,1,16,256]{4,3,2,1,0:T(8,128)(2,1)} %convert_bitcast_fusion), calls=%async_computation.4 | async-start | bytes 2097152 | tf_op jit(solution)/shard_map/all_to_all | solution.py:28
  503.3 78.7 %all-to-all-start.1 = ((bf16[16,8,12,2048]{3,0,2,1:T(8,128)(2,1)}), bf16[16,8,12,2048]{3,0,2,1:T(8,128)(2,1)}, u32[]{:S(2)}, u32[]{:S(2)}) async-start(bf16[16,8,12,2048]{3,0,2,1:T(8,128)(2,1)} %copy.76), calls=%async_computation.1 | async-start | bytes 12582912 | tf_op jit(solution)/shard_map/all_to_all | solution.py:120
  631.5 10.3 copy-start.2
  631.5 10.3 copy-start.3
  631.5 10.3 copy-start.7
  631.5 28.0 %copy-start.5 = (f32[16,256]{1,0:T(8,128)S(1)}, f32[16,256]{1,0:T(8,128)}, u32[]{:S(2)}) copy-start(f32[16,256]{1,0:T(8,128)} %param.19) | copy-start | bytes 49156
  631.5 43.7 %copy-start.6 = (f32[128,8]{0,1:T(8,128)S(1)}, f32[128,8]{0,1:T(8,128)}, u32[]{:S(2)}) copy-start(f32[128,8]{0,1:T(8,128)} %param.12) | copy-start | bytes 12292
  631.6 405.9 %all-to-all-start.5 = ((bf16[128,1,1,12,2048]{4,3,2,1,0:T(8,128)(2,1)}), bf16[128,1,1,12,2048]{4,3,2,1,0:T(8,128)(2,1)}, u32[]{:S(2)}, u32[]{:S(2)}) async-start(bf16[128,1,1,12,2048]{4,3,2,1,0:T(8,128)(2,1)} %bitcast.78), calls=%async_computation.5 | async-start | bytes 16777216 | tf_op jit(solution)/shard_map/all_to_all | solution.py:28
  641.7 207.5 %all-gather.3.cloned.1.call-start = ((), (), s32[]{:S(2)}) async-start(), calls=%async_computation.6 | async-start | bytes 2228224 | tf_op jit(solution)/shard_map/all_gather | solution.py:39
  659.5 407.5 %all-gather.5.cloned.1.call-start = ((), (), s32[]{:S(2)}) async-start(), calls=%async_computation.7 | async-start | bytes 1114112 | tf_op jit(solution)/shard_map/all_gather | solution.py:149
  1060.5 9.8 copy-start.1
Sparse Core Ops, SparseCore 0:
  659.6 189.5 all-gather.2
  851.0 111.1 all-gather.4
where the time goes:
time: 1090 us; the launch traced here: 1080 us
  waiting for transfers between devices  745 us (68%)
  local copies, waits for them, and re-layouts  113 us (10%)
  blocking collectives  113 us (10%)
  starting transfers between devices  54.5 us (5%)
  matrix products  23.4 us (2%)
  other arithmetic  14.6 us (1%)
  between operations  14.6 us (1%)
    all_to_all x1, waiting for transfers between devices, on_device(): lax.all_to_all(outbox.reshape(fs_count, tp_count, capacity, width), 'fs',...  269 us
    all_to_all x3, waiting for transfers between devices, joined_exchange(): tiles = lax.all_to_all(tiles, axis, split_axis=0, concat_axis=0, tiled=True)  241 us
    all_gather x1, waiting for transfers between devices, side_by_side(): lax.all_gather(both, axis, axis=dim, tiled=True)  174 us
    all_to_all x1, blocking collectives, joined_exchange(): tiles = lax.all_to_all(tiles, axis, split_axis=0, concat_axis=0, tiled=True)  81.9 us
    all_to_all x1, waiting for transfers between devices, on_device(): lax.all_to_all(lax.all_to_all(outbox.reshape(fs_count, tp_count, capacity...  60.4 us
    all_to_all x3, starting transfers between devices, joined_exchange(): tiles = lax.all_to_all(tiles, axis, split_axis=0, concat_axis=0, tiled=True)  39 us
  transfers between devices with their start and end apart: 7, of which 6 were waited for; matrix products, arithmetic and copies ran while one was open for 9% of the time, Pallas kernels for 0%

commit v1 on v0

v1 whole, which is shorter than its diff:
```python
import functools

import jax
import jax.numpy as jnp
import numpy as np
from jax import lax
from jax.experimental import pallas as pl
from jax.experimental.pallas import tpu as pltpu
from jax.sharding import PartitionSpec as P

EPSILON = 1e-06
route_scale = 2.5
ABSENT = -1024.0
MESH = pl.DeviceIdType.MESH
GROUP = 4
AG_PIECES = 2
RS_PIECES = 4
VMEM = pl.BlockSpec(memory_space=pltpu.VMEM)


def slot_of(offset):
    return 2 * offset if offset >= 0 else -2 * offset - 1


def greet(names_and_counts):
    barrier = pltpu.get_barrier_semaphore()
    total = 0
    for name, steps in names_and_counts:
        size = lax.axis_size(name)
        me = lax.axis_index(name)
        for step in steps:
            peer = lax.rem(me + step + size, size)
            pl.semaphore_signal(barrier, inc=1, device_id={name: peer}, device_id_type=MESH)
            total += 1
    return barrier, total


def remote(src, dst, send, recv, name, peer):
    return pltpu.make_async_remote_copy(
        src_ref=src, dst_ref=dst, send_sem=send, recv_sem=recv,
        device_id={name: peer}, device_id_type=MESH,
    )


def dispatch_kernel(
    n, m, cap, tok_ref, ids_ref, sc_ref, sgu_ref, sd_ref,
    x_ref, cw_ref, h_ref, hgu_ref, hd_ref,
    all_ref, meta_ref, stage_ref, pick_ref, gs_ref,
    ag_send, ag_recv, meta_send, meta_recv, x_send, x_recv, own_sem,
    gu_send, gu_recv, sd_send, sd_recv, gs_send, gs_recv,
):
    z, tp = lax.axis_index("fs"), lax.axis_index("tp")
    rows, width = tok_ref.shape
    picks = ids_ref.shape[0]
    up, down = lax.rem(z + 1, n), lax.rem(z + n - 1, n)
    wide = min(512, width)
    slots = GROUP * cap
    cols_f = sgu_ref.shape[1]
    own_h = gs_ref.shape[1]

    barrier, arrivals = greet((("fs", range(1, n)), ("tp", range(1, m))))
    widened = tok_ref[...].astype(jnp.float32)
    scale = lax.rsqrt(jnp.mean(widened * widened, axis=1, keepdims=True) + EPSILON)
    all_ref[pl.ds(0, rows), :] = (widened * scale).astype(jnp.bfloat16)
    scores = sc_ref[...]
    meta_ref[0, pl.ds(0, picks), :] = ids_ref[...].astype(jnp.float32)
    meta_ref[0, pl.ds(picks, picks), :] = route_scale * scores / jnp.sum(scores, axis=0, keepdims=True)
    hgu_ref[:, pl.ds(pl.multiple_of(tp * cols_f, cols_f), cols_f), :] = sgu_ref[...]
    hd_ref[:, pl.ds(pl.multiple_of(tp * sd_ref.shape[1], 128), sd_ref.shape[1])] = sd_ref[...]
    pl.semaphore_wait(barrier, arrivals)

    step_rows = rows // AG_PIECES

    def ring(k, p):
        src = max(k - 2, 0)
        peer = up if k % 2 == 1 else down
        return remote(
            all_ref.at[pl.ds(src * rows + p * step_rows, step_rows), :],
            all_ref.at[pl.ds(k * rows + p * step_rows, step_rows), :],
            ag_send.at[k, p], ag_recv.at[k, p], "fs", peer,
        )

    def ring_meta(k):
        peer = up if k % 2 == 1 else down
        return remote(meta_ref.at[max(k - 2, 0)], meta_ref.at[k], meta_send.at[k], meta_recv.at[k], "fs", peer)

    def gather_gu(q):
        return remote(
            sgu_ref,
            hgu_ref.at[:, pl.ds(pl.multiple_of(tp * cols_f, cols_f), cols_f), :],
            gu_send.at[q - 1], gu_recv.at[q - 1], "tp", lax.rem(tp + q, m),
        )

    def gather_sd(q):
        return remote(
            sd_ref,
            hd_ref.at[:, pl.ds(pl.multiple_of(tp * sd_ref.shape[1], 128), sd_ref.shape[1])],
            sd_send.at[q - 1], sd_recv.at[q - 1], "tp", lax.rem(tp + q, m),
        )

    def slice_gs(r):
        peer = lax.rem(z + r, n)
        return remote(
            hgu_ref.at[:, pl.ds(pl.multiple_of(peer * own_h, own_h), own_h), :],
            gs_ref.at[:, :, pl.ds(pl.multiple_of(z * 128, 128), 128)],
            gs_send.at[r - 1], gs_recv.at[r - 1], "fs", peer,
        )

    def exchange(g, q):
        peer = lax.rem(tp + q, m)
        return remote(stage_ref.at[g, peer], x_ref.at[g, tp], x_send.at[g, q - 1], x_recv.at[g, q - 1], "tp", peer)

    def own(g):
        return pltpu.make_async_copy(stage_ref.at[g, tp], x_ref.at[g, tp], own_sem.at[g])

    for k in (1, 2):
        ring_meta(k).start()
        for p in range(AG_PIECES):
            ring(k, p).start()
    for q in range(1, m):
        gather_gu(q).start()
        gather_sd(q).start()
    for q in range(1, m):
        gather_gu(q).wait_recv()
    for r in range(1, n):
        slice_gs(r).start()
    gs_ref[:, :, pl.ds(pl.multiple_of(z * 128, 128), 128)] = hgu_ref[
        :, pl.ds(pl.multiple_of(z * own_h, own_h), own_h), :
    ]

    before = lax.broadcasted_iota(jnp.int32, (rows, rows), 0) < lax.broadcasted_iota(jnp.int32, (rows, rows), 1)
    before = before.astype(jnp.float32).astype(jnp.bfloat16)
    served = (lax.broadcasted_iota(jnp.int32, (m, rows), 0) + m * z).astype(jnp.float32)
    places = lax.broadcasted_iota(jnp.int32, (slots, rows), 0).astype(jnp.float32)

    def select(g):
        for b in range(GROUP):
            k = g * GROUP + b
            meta = meta_ref[k]
            chosen = jnp.zeros((m, rows), jnp.float32)
            weight = jnp.zeros((m, rows), jnp.float32)
            for j in range(picks):
                hit = meta[j : j + 1, :] == served
                chosen = chosen + hit.astype(jnp.float32)
                weight = weight + jnp.where(hit, meta[picks + j : picks + j + 1, :], 0.0)
            rank = jnp.dot(chosen.astype(jnp.bfloat16), before, preferred_element_type=jnp.float32)
            code = jnp.where(chosen > 0.0, rank, ABSENT)
            cw_ref[k, pl.ds(0, m), :] = code
            cw_ref[k, pl.ds(m, m), :] = weight
            for q in range(m):
                hot = (jnp.broadcast_to(code[q : q + 1, :], (slots, rows)) + float(cap * b)) == places
                pick_ref[pl.ds(q * slots, slots), pl.ds(b * rows, rows)] = hot.astype(jnp.float32).astype(jnp.bfloat16)

        @pl.loop(0, width // wide)
        def _(c):
            cols = pl.ds(pl.multiple_of(c * wide, wide), wide)
            taken = jnp.dot(
                pick_ref[...], all_ref[pl.ds(g * GROUP * rows, GROUP * rows), cols],
                preferred_element_type=jnp.float32,
            ).astype(jnp.bfloat16)
            stage_ref[g, :, :, cols] = taken.reshape(m, slots, wide)

        for q in range(1, m):
            exchange(g, q).start()
        own(g).start()

    for k in range(1, n):
        ring_meta(k).wait_recv()
        if k + 2 < n:
            ring_meta(k + 2).start()
        for p in range(AG_PIECES):
            ring(k, p).wait_recv()
            if k + 2 < n:
                ring(k + 2, p).start()
        if k % GROUP == GROUP - 1:
            select(k // GROUP)

    for r in range(1, n):
        slice_gs(r).wait_recv()
    for g in range(n // GROUP):
        some = pl.ds(g * GROUP * rows, GROUP * rows)
        both = lax.dot_general(
            all_ref[some, :], gs_ref[...].reshape(2 * own_h, width), (((1,), (1,)), ((), ())),
            preferred_element_type=jnp.float32,
        )
        gate, upper = both[:, :own_h], both[:, own_h:]
        h_ref[some, :] = (gate / (1.0 + jnp.exp(-gate)) * upper).astype(jnp.bfloat16)

    for q in range(1, m):
        gather_gu(q).wait_send()
        gather_sd(q).wait()
    for r in range(1, n):
        slice_gs(r).wait_send()
    for k in range(1, n):
        ring_meta(k).wait_send()
        for p in range(AG_PIECES):
            ring(k, p).wait_send()
    for g in range(n // GROUP):
        own(g).wait()
        for q in range(1, m):
            exchange(g, q).wait()


def combine_kernel(
    n, m, cap, x_ref, gate_ref, up_ref, down_ref, cw_ref, h_ref, sd_ref, ecode_ref, ew_ref, place_ref,
    out_ref,
    y_ref, rv_ref, c_ref, d_ref, pin_ref, min_ref, pst_ref, mst_ref,
    y_send, y_recv, own_sem, p_send, p_recv, m_send, m_recv,
):
    z, tp = lax.axis_index("fs"), lax.axis_index("tp")
    rows, width = out_ref.shape
    upward, downward = lax.rem(z + 1, n), lax.rem(z + n - 1, n)
    wide = min(512, width)
    slots = GROUP * cap
    lanes = m * slots
    half = n // 2
    groups = n // GROUP
    part = rows // RS_PIECES

    barrier, arrivals = greet((("fs", (1, -1)), ("tp", range(1, m))))
    pl.semaphore_wait(barrier, arrivals)

    def exchange(g, q):
        peer = lax.rem(tp + q, m)
        return remote(y_ref.at[g, peer], rv_ref.at[g, tp], y_send.at[g, q - 1], y_recv.at[g, q - 1], "tp", peer)

    def own(g):
        return pltpu.make_async_copy(y_ref.at[g, tp], rv_ref.at[g, tp], own_sem.at[g])

    @pl.loop(0, groups)
    def _(i):
        g = groups - 1 - i
        x = x_ref[g]
        gate = jnp.dot(x, gate_ref[...], preferred_element_type=jnp.float32)
        upper = jnp.dot(x, up_ref[...], preferred_element_type=jnp.float32)
        hidden = (gate / (1.0 + jnp.exp(-gate)) * upper).astype(jnp.bfloat16)

        @pl.loop(0, width // wide)
        def _(c):
            cols = pl.ds(pl.multiple_of(c * wide, wide), wide)
            y = jnp.dot(hidden, down_ref[:, cols], preferred_element_type=jnp.float32)
            y_ref[g, :, :, cols] = y.astype(jnp.bfloat16).reshape(m, slots, wide)

        for q in range(1, m):
            exchange(g, q).start()
        own(g).start()

    def combine(g):
        own(g).wait()
        for q in range(1, m):
            exchange(g, q).wait_recv()
        some = pl.ds(g * GROUP * rows, GROUP * rows)
        exact = cw_ref[some, :]
        high = exact.astype(jnp.bfloat16)
        low = (exact - high.astype(jnp.float32)).astype(jnp.bfloat16)
        code = jnp.dot(high, ecode_ref[...], preferred_element_type=jnp.float32)
        high = jnp.dot(high, ew_ref[...], preferred_element_type=jnp.float32)
        low = jnp.dot(low, ew_ref[...], preferred_element_type=jnp.float32)
        for b in range(GROUP):
            span = slice(b * rows, (b + 1) * rows)
            hit = (code[span] + float(cap * b)) == place_ref[...]
            c_ref[pl.ds(b * rows, rows), pl.ds(0, lanes)] = jnp.where(hit, high[span], 0.0).astype(jnp.bfloat16)
            c_ref[pl.ds(b * rows, rows), pl.ds(lanes, lanes)] = jnp.where(hit, low[span], 0.0).astype(jnp.bfloat16)

        @pl.loop(0, width // wide)
        def _(c):
            cols = pl.ds(pl.multiple_of(c * wide, wide), wide)
            back = rv_ref[g, :, :, cols].reshape(lanes, wide)
            total = jnp.dot(c_ref[:, pl.ds(0, lanes)], back, preferred_element_type=jnp.float32)
            total += jnp.dot(c_ref[:, pl.ds(lanes, lanes)], back, preferred_element_type=jnp.float32)
            total += jnp.dot(h_ref[some, :], sd_ref[:, cols], preferred_element_type=jnp.float32)
            d_ref[g % 2, :, cols] = total

    def share(offset, c):
        k = slot_of(offset)
        return d_ref[(k // GROUP) % 2, pl.ds((k % GROUP) * rows + c * part, part), :]

    def hop(sign, r, c):
        some = pl.ds(c * part, part)
        if sign > 0:
            return remote(pst_ref.at[r - 1, some, :], pin_ref.at[r - 1, some, :],
                          p_send.at[r - 1, c], p_recv.at[r - 1, c], "fs", upward)
        return remote(mst_ref.at[r - 1, some, :], min_ref.at[r - 1, some, :],
                      m_send.at[r - 1, c], m_recv.at[r - 1, c], "fs", downward)

    def forward(sign, r, c):
        some = pl.ds(c * part, part)
        total = share(sign * r, c)
        if r < (half - 1 if sign > 0 else half):
            hop(sign, r + 1, c).wait_recv()
            total = total + (pin_ref if sign > 0 else min_ref)[r, some, :].astype(jnp.float32)
        (pst_ref if sign > 0 else mst_ref)[r - 1, some, :] = total.astype(jnp.bfloat16)
        hop(sign, r, c).start()

    combine(groups - 1)
    for i in range(half):
        for c in range(RS_PIECES):
            forward(-1, half - i, c)
            if half - 1 - i > 0:
                forward(1, half - 1 - i, c)
        if i % 2 == 0 and groups - 2 - i // 2 >= 0:
            combine(groups - 2 - i // 2)
    for c in range(RS_PIECES):
        some = pl.ds(c * part, part)
        hop(1, 1, c).wait_recv()
        hop(-1, 1, c).wait_recv()
        total = share(0, c) + pin_ref[0, some, :].astype(jnp.float32) + min_ref[0, some, :].astype(jnp.float32)
        out_ref[some, :] = total.astype(jnp.bfloat16)

    for c in range(RS_PIECES):
        for r in range(1, half):
            hop(1, r, c).wait_send()
        for r in range(1, half + 1):
            hop(-1, r, c).wait_send()
    for g in range(groups):
        for q in range(1, m):
            exchange(g, q).wait_send()


def on_device(
    tokens, route_ids, route_scores, norm_gain,
    expert_gate, expert_up, expert_down, shared_gate, shared_up, shared_down,
):
    n = lax.axis_size("fs")
    m = lax.axis_size("tp")
    experts = n * m
    rows, width = tokens.shape
    picks = route_ids.shape[1]
    cap = 3 * rows * picks // (2 * experts)
    slots = GROUP * cap
    groups = n // GROUP
    half = n // 2
    bf16, f32 = jnp.bfloat16, jnp.float32
    dma = pltpu.SemaphoreType.DMA

    deep, cols_f = expert_gate.shape[1:]
    down_rows, down_cols = expert_down.shape[1:]
    gate_t = (norm_gain[None, None, :] * jnp.swapaxes(expert_gate, 1, 2)).astype(bf16)
    up_t = (norm_gain[None, None, :] * jnp.swapaxes(expert_up, 1, 2)).astype(bf16)
    halves = down_cols // deep
    down_t = jnp.swapaxes(expert_down.astype(bf16).reshape(experts, down_rows, halves, deep), 1, 2)
    packed = jnp.concatenate([gate_t, up_t, down_t.reshape(experts, halves * down_rows, deep)], axis=1)
    moved = lax.all_to_all(packed, ("fs", "tp"), split_axis=0, concat_axis=0, tiled=True)
    moved = moved.reshape(n, m, packed.shape[1], deep)

    def served(tile):
        return jnp.transpose(tile, (0, 3, 1, 2)).reshape(n * deep, m * cols_f)

    served_gate = served(moved[:, :, :cols_f])
    served_up = served(moved[:, :, cols_f : 2 * cols_f])
    served_down = jnp.transpose(
        moved[:, :, 2 * cols_f :].reshape(n, m, halves, down_rows, deep), (0, 3, 1, 2, 4)
    ).reshape(n * down_rows, m * down_cols)

    shared_t = jnp.stack([
        (norm_gain[None, :] * shared_gate.T).astype(bf16), (norm_gain[None, :] * shared_up.T).astype(bf16),
    ])
    own_h = m * cols_f // n
    routed, codes, hidden, held_gu, held_down = pl.pallas_call(
        functools.partial(dispatch_kernel, n, m, cap),
        out_shape=(
            jax.ShapeDtypeStruct((groups, m, slots, width), bf16),
            jax.ShapeDtypeStruct((n, 2 * m, rows), f32),
            jax.ShapeDtypeStruct((n * rows, own_h), bf16),
            jax.ShapeDtypeStruct((2, m * cols_f, deep), bf16),
            jax.ShapeDtypeStruct((down_rows, m * down_cols), bf16),
        ),
        in_specs=[VMEM] * 5,
        out_specs=(VMEM,) * 5,
        scratch_shapes=[
            pltpu.VMEM((n * rows, width), bf16),
            pltpu.VMEM((n, 2 * picks, rows), f32),
            pltpu.VMEM((groups, m, slots, width), bf16),
            pltpu.VMEM((m * slots, GROUP * rows), bf16),
            pltpu.VMEM((2, own_h, width), bf16),
            dma((n, AG_PIECES)), dma((n, AG_PIECES)), dma((n,)), dma((n,)),
            dma((groups, m - 1)), dma((groups, m - 1)), dma((groups,)),
            dma((m - 1,)), dma((m - 1,)), dma((m - 1,)), dma((m - 1,)), dma((n - 1,)), dma((n - 1,)),
        ],
        compiler_params=pltpu.CompilerParams(
            collective_id=0, has_side_effects=True, vmem_limit_bytes=48 * 1024 * 1024,
        ),
        cost_estimate=pl.CostEstimate(flops=100_000_000_000, bytes_accessed=30_000_000, transcendentals=0),
        name="dispatch",
    )(tokens, route_ids.T, route_scores.T, shared_t, shared_down.astype(bf16))

    lane = np.arange(m * slots)
    expand = (lane[None, :] // slots == np.arange(2 * m)[:, None]).astype(np.float32)
    ecode = jnp.asarray(expand, bf16)
    ew = jnp.asarray(np.roll(expand, m, axis=0), bf16)
    place = jnp.asarray((lane % slots)[None, :].astype(np.float32))
    codes = jnp.transpose(codes, (0, 2, 1)).reshape(n * rows, 2 * m)
    mixed = pl.pallas_call(
        functools.partial(combine_kernel, n, m, cap),
        out_shape=jax.ShapeDtypeStruct((rows, width), bf16),
        in_specs=[VMEM] * 10,
        out_specs=VMEM,
        scratch_shapes=[
            pltpu.VMEM((groups, m, slots, width), bf16),
            pltpu.VMEM((groups, m, slots, width), bf16),
            pltpu.VMEM((GROUP * rows, 2 * m * slots), bf16),
            pltpu.VMEM((2, GROUP * rows, width), f32),
            pltpu.VMEM((half - 1, rows, width), bf16),
            pltpu.VMEM((half, rows, width), bf16),
            pltpu.VMEM((half - 1, rows, width), bf16),
            pltpu.VMEM((half, rows, width), bf16),
            dma((groups, m - 1)), dma((groups, m - 1)), dma((groups,)),
            dma((half - 1, RS_PIECES)), dma((half - 1, RS_PIECES)),
            dma((half, RS_PIECES)), dma((half, RS_PIECES)),
        ],
        compiler_params=pltpu.CompilerParams(
            collective_id=1, has_side_effects=True, vmem_limit_bytes=60 * 1024 * 1024,
        ),
        cost_estimate=pl.CostEstimate(flops=100_000_000_000, bytes_accessed=30_000_000, transcendentals=0),
        name="combine",
    )(
        routed.reshape(groups, m * slots, width), served_gate, served_up, served_down, codes, hidden, held_down,
        ecode, ew, place,
    )
    return (
        mixed, served_gate[None], served_up[None], served_down[None],
        held_gu[0].T, held_gu[1].T, held_down,
    )


def solution(mesh):
    return jax.shard_map(
        on_device,
        mesh=mesh,
        in_specs=(
            P(("grp", "fs", "tp"), None),
            P(("grp", "fs", "tp"), None),
            P(("grp", "fs", "tp"), None),
            P("fs"),
            P(None, "fs", "tp"),
            P(None, "fs", "tp"),
            P(None, "fs", "tp"),
            P("fs", "tp"),
            P("fs", "tp"),
            P("fs", "tp"),
        ),
        out_specs=(
            P(("grp", "fs", "tp"), None),
            P(("grp", "fs", "tp"), None, None),
            P(("grp", "fs", "tp"), None, None),
            P(("grp", "fs", "tp"), None, None),
            P(("grp", "fs"), None),
            P(("grp", "fs"), None),
            P(("grp", "fs"), None),
        ),
        check_vma=False,
    )
```

time: 1090 us -> 453 us (0.42); the launches traced: 1080 us -> 452 us
  waiting for transfers between devices: 745 us -> 0.01 us
  Pallas kernels: 0 us -> 388 us
  blocking collectives: 113 us -> 0 us
  local copies, waits for them, and re-layouts: 113 us -> 26.6 us
  matrix products: 23.4 us -> 0 us
  starting transfers between devices: 54.5 us -> 31.2 us
  between operations: 14.6 us -> 0.87 us
    all_to_all x5 -> x1, waiting for transfers between devices: 571 us -> 0.01 us  [on_device(): lax.all_to_all(packed, ('fs', 'tp'), split_axis=0, concat_axis=0, tiled=T...]
    pallas_call x0 -> x2, Pallas kernels: none -> 388 us  [the longest x1 261 us: on_device(): pl.pallas_call(functools.partial(dispatch_kernel, n, m, cap), out_shape=(...]
    all_gather x2 -> x0, waiting for transfers between devices: 174 us -> none  [the longest x1 174 us: side_by_side(): lax.all_gather(both, axis, axis=dim, tiled=True)]
    all_to_all x1 -> x0, blocking collectives: 81.9 us -> none  [joined_exchange(): tiles = lax.all_to_all(tiles, axis, split_axis=0, concat_axis=0, tiled=True)]
    reshape x7 -> x4, local copies, waits for them, and re-layouts: 38.5 us -> 5.51 us  [the longest x2 3.56 us: served(): return jnp.transpose(tile, (0, 3, 1, 2)).reshape(n * deep, m * cols_f)]
    all_gather x2 -> x0, blocking collectives: 30.9 us -> none  [the longest x1 16.9 us: side_by_side(): lax.all_gather(both, axis, axis=dim, tiled=True)]
    dot_general x4 -> x0, matrix products: 23.4 us -> none  [the longest x1 12.6 us: expert_rows(): jnp.dot(hidden, w_down, preferred_element_type=jnp.float32)]
    all_to_all x5 -> x1, starting transfers between devices: 54.3 us -> 31.2 us  [on_device(): lax.all_to_all(packed, ('fs', 'tp'), split_axis=0, concat_axis=0, tiled=T...]
  transfers between devices with their start and end apart: 7 -> 1, of which waited for: 6 -> 0; matrix products, arithmetic and copies ran while one was open for 9% -> 1% of each run, Pallas kernels for 0% -> 58%
where the time goes in v1:
time: 453 us; the launch traced here: 452 us
  Pallas kernels  388 us (86%)
  starting transfers between devices  31.2 us (7%)
  local copies, waits for them, and re-layouts  26.6 us (6%)
  other arithmetic  5.63 us (1%)
    pallas_call x1, Pallas kernels, on_device(): pl.pallas_call(functools.partial(dispatch_kernel, n, m, cap), out_shape=(...  261 us
    pallas_call x1, Pallas kernels, on_device(): pl.pallas_call(functools.partial(combine_kernel, n, m, cap), out_shape=ja...  127 us
    all_to_all x1, starting transfers between devices, on_device(): lax.all_to_all(packed, ('fs', 'tp'), split_axis=0, concat_axis=0, tiled=T...  31.2 us
    unnamed x32, local copies, waits for them, and re-layouts  9.89 us
  transfers between devices with their start and end apart: 1, of which 0 were waited for; matrix products, arithmetic and copies ran while one was open for 1% of the time, Pallas kernels for 58%

profile of v1, /device:TPU:33, one launch (start us, length us, event | category | flops | bytes accessed | tf_op | source)
XLA Modules:
  0.0 452.3 jit_solution(9818742687752635168)
XLA Ops:
  0.6 0.0 copy-start.11
  0.6 1.7 convert_element_type.39
  2.4 0.3 reshape.44
  2.7 0.0 copy-start.6
  2.7 0.2 copy.39
  2.9 0.0 copy-done.11
  2.9 1.4 copy-done.6
  4.3 2.1 fusion
  6.4 1.8 pad_maximum_fusion
  8.2 0.0 copy-start.10
  8.2 0.0 copy-start.3
  8.2 0.0 copy-start.4
  8.2 31.2 %all-to-all-start = ((bf16[128,96,128]{2,1,0:T(8,128)(2,1)}), bf16[128,96,128]{2,1,0:T(8,128)(2,1)}, u32[]{:S(2)}, u32[]{:S(2)}) async-start(bf16[128,96,128]{2,1,0:T(8,128)(2,1)} %pad_maximum_fusion), calls=%async_computation | async-start | bytes 6291456 | tf_op jit(solution)/shard_map/all_to_all | solution.py:343
  39.4 0.0 copy-done.10
  39.4 0.0 copy-done.8
  39.5 0.0 copy-done.9
  39.5 0.0 copy-done.2
  39.5 0.0 copy-done.3
  39.5 0.0 copy-done.4
  39.5 261.2 %dispatch.1 = (bf16[4,8,48,2048]{3,2,1,0:T(8,128)(2,1)}, f32[16,16,128]{2,1,0:T(8,128)S(1)}, bf16[2048,16]{1,0:T(8,128)(2,1)S(1)}, bf16[2,256,128]{2,1,0:T(8,128)(2,1)S(1)}, bf16[16,2048]{1,0:T(8,128)(2,1)S(1)}) custom-call(bf16[128,2048]{1,0:T(8,128)(2,1)S(1)} %copy-done.2, s32[8,128]{1,0:T(8,128)S(1)} %bitcast.58, f32[8,128]{1,0:T(8,128)S(1)} %bitcast.59, ...), custom_call_target="tpu_custom_call" | custom-call | flops 99999997952 | bytes 30000000 | tf_op jit(solution)/shard_map/dispatch/pallas_call | solution.py:359
  300.7 0.0 copy-start
  300.7 0.6 copy-done
  301.3 0.8 copy-done.5
  302.1 1.4 copy.43
  303.5 0.7 copy.51
  304.3 0.7 copy.52
  305.0 0.0 all-to-all-done
  305.0 3.6 fusion.4
  308.6 1.0 copy.42
  309.5 1.7 reshape.50.down_ref
  311.2 1.6 broadcast_in_dim_reshape.11
  312.8 0.7 copy.40
  313.5 0.5 broadcast_in_dim_reshape.9
  314.0 0.3 copy.58
  314.3 1.3 copy.44.gate_ref
  315.6 1.9 copy.41
  317.5 0.5 broadcast_in_dim_reshape.10
  318.0 1.2 copy.57
  319.2 2.3 copy.45.up_ref
  321.5 126.8 %combine.1 = bf16[128,2048]{1,0:T(8,128)(2,1)} custom-call(bf16[4,384,2048]{2,1,0:T(8,128)(2,1)} %bitcast.68, bf16[2048,256]{1,0:T(8,128)(2,1)} %copy.44.gate_ref, bf16[2048,256]{1,0:T(8,128)(2,1)} %copy.45.up_ref, bf16[256,2048]{1,0:T(8,128)(2,1)} %reshape.50.down_ref, f32[2048,16]{1,0:T(8,128)} %bitcast.67, bf16[2048,16]{1,0:T(8,128)(2,1)} %copy-done.5, ...), custom_call_target="tpu_custom_call" | custom-call | flops 99999997952 | bytes 30000000 | tf_op jit(solution)/shard_map/combine/pallas_call | solution.py:393
  448.2 0.0 copy-start.7
  448.2 0.0 copy-start.1
  448.3 1.3 copy.49
  449.6 1.3 copy.50
  450.9 0.0 copy-done.7
  450.9 0.8 copy.61
  451.7 0.0 copy-done.1
  451.7 0.6 copy.62
  (8 shorter events, 0.0 us)
Async XLA Ops:
  0.6 2.2 copy-start.11
  2.7 1.6 copy-start.6
  8.2 31.3 %copy-start.10 = (f32[16,256]{1,0:T(8,128)S(1)}, f32[16,256]{1,0:T(8,128)}, u32[]{:S(2)}) copy-start(f32[16,256]{1,0:T(8,128)} %param.22) | copy-start | bytes 49156
  8.2 31.3 %copy-start.8 = (f32[128,32]{0,1:T(8,128)S(1)}, f32[128,32]{0,1:T(8,128)}, u32[]{:S(2)}) copy-start(f32[128,32]{0,1:T(8,128)} %param.20) | copy-start | bytes 49156
  8.2 31.3 %copy-start.9 = (f32[128,32]{0,1:T(8,128)S(1)}, f32[128,32]{0,1:T(8,128)}, u32[]{:S(2)}) copy-start(f32[128,32]{0,1:T(8,128)} %param.21) | copy-start | bytes 49156
  8.2 31.3 %copy-start.2 = (bf16[128,2048]{1,0:T(8,128)(2,1)S(1)}, bf16[128,2048]{1,0:T(8,128)(2,1)}, u32[]{:S(2)}) copy-start(bf16[128,2048]{1,0:T(8,128)(2,1)} %tok_ref.1) | copy-start | bytes 1572868
  8.2 31.3 %copy-start.3 = (s32[128,8]{0,1:T(8,128)S(1)}, s32[128,8]{0,1:T(8,128)}, u32[]{:S(2)}) copy-start(s32[128,8]{0,1:T(8,128)} %param.14) | copy-start | bytes 12292
  8.2 31.3 %copy-start.4 = (f32[128,8]{0,1:T(8,128)S(1)}, f32[128,8]{0,1:T(8,128)}, u32[]{:S(2)}) copy-start(f32[128,8]{0,1:T(8,128)} %param.15) | copy-start | bytes 12292
  8.2 296.8 %all-to-all-start = ((bf16[128,96,128]{2,1,0:T(8,128)(2,1)}), bf16[128,96,128]{2,1,0:T(8,128)(2,1)}, u32[]{:S(2)}, u32[]{:S(2)}) async-start(bf16[128,96,128]{2,1,0:T(8,128)(2,1)} %pad_maximum_fusion), calls=%async_computation | async-start | bytes 6291456 | tf_op jit(solution)/shard_map/all_to_all | solution.py:343
  300.7 0.6 copy-start
  301.3 0.8 copy-start.5
  448.2 2.6 copy-start.7
  448.2 3.4 copy-start.1

commit v2 on v1

v2 whole, which is shorter than its diff:
```python
import functools

import jax
import jax.numpy as jnp
import numpy as np
from jax import lax
from jax.experimental import pallas as pl
from jax.experimental.pallas import tpu as pltpu
from jax.sharding import PartitionSpec as P

EPSILON = 1e-06
route_scale = 2.5
ABSENT = -1024.0
MESH = pl.DeviceIdType.MESH
GROUP = 4
AG_PIECES = 2
W_FIRST, W_EVERY = 5, 4
VMEM = pl.BlockSpec(memory_space=pltpu.VMEM)


def slot_of(offset):
    return 2 * offset if offset >= 0 else -2 * offset - 1


def greet(names_and_counts):
    barrier = pltpu.get_barrier_semaphore()
    total = 0
    for name, steps in names_and_counts:
        size = lax.axis_size(name)
        me = lax.axis_index(name)
        for step in steps:
            peer = lax.rem(me + step + size, size)
            pl.semaphore_signal(barrier, inc=1, device_id={name: peer}, device_id_type=MESH)
            total += 1
    return barrier, total


def remote(src, dst, send, recv, name, peer):
    return pltpu.make_async_remote_copy(
        src_ref=src, dst_ref=dst, send_sem=send, recv_sem=recv,
        device_id={name: peer}, device_id_type=MESH,
    )


def offset_of(slot):
    return slot // 2 if slot % 2 == 0 else -((slot + 1) // 2)


def kernel(
    n, m, cap, tok_ref, ids_ref, sc_ref, sgu_ref, sd_ref, wg_ref, wu_ref, wd_ref, ecode_ref, ew_ref, place_ref,
    out_ref, gate_ref, up_ref, down_ref, hgu_ref, hd_ref,
    all_ref, meta_ref, cw_ref, stage_ref, x_ref, rv_ref, pick_ref, gs_ref, h_ref,
    mg_ref, mu_ref, md_ref, fg_ref, fu_ref, fd_ref, c_ref, d_ref, pin_ref, min_ref, pst_ref, mst_ref,
    ag_send, ag_recv, meta_send, meta_recv, x_send, x_recv, y_send, y_recv,
    gu_send, gu_recv, sd_send, sd_recv, gs_send, gs_recv,
    wz_send, wz_recv, wz_own, wx_send, wx_recv, p_send, p_recv, m_send, m_recv,
):
    z, tp = lax.axis_index("fs"), lax.axis_index("tp")
    rows, width = tok_ref.shape
    picks = ids_ref.shape[0]
    above, below = lax.rem(z + 1, n), lax.rem(z + n - 1, n)
    parts, wide = stage_ref.shape[1], stage_ref.shape[4]
    slots = GROUP * cap
    lanes = m * slots
    half, groups = n // 2, n // GROUP
    cols_f, deep = sgu_ref.shape[1:]
    own_h = gs_ref.shape[1]
    down_rows, down_cols = sd_ref.shape

    def tp_rows(size):
        return pl.ds(pl.multiple_of(tp * size, size), size)

    barrier, arrivals = greet((("fs", range(1, n)), ("tp", range(1, m))))
    widened = tok_ref[...].astype(jnp.float32)
    scale = lax.rsqrt(jnp.mean(widened * widened, axis=1, keepdims=True) + EPSILON)
    all_ref[pl.ds(0, rows), :] = (widened * scale).astype(jnp.bfloat16)
    scores = sc_ref[...]
    meta_ref[0, pl.ds(0, picks), :] = ids_ref[...].astype(jnp.float32)
    meta_ref[0, pl.ds(picks, picks), :] = route_scale * scores / jnp.sum(scores, axis=0, keepdims=True)
    hgu_ref[:, tp_rows(cols_f), :] = sgu_ref[...]
    hd_ref[:, tp_rows(down_cols)] = sd_ref[...]
    pl.semaphore_wait(barrier, arrivals)

    step_rows = rows // AG_PIECES

    def ring(k, p):
        src = max(k - 2, 0)
        return remote(
            all_ref.at[pl.ds(src * rows + p * step_rows, step_rows), :],
            all_ref.at[pl.ds(k * rows + p * step_rows, step_rows), :],
            ag_send.at[k, p], ag_recv.at[k, p], "fs", above if k % 2 == 1 else below,
        )

    def ring_meta(k):
        return remote(
            meta_ref.at[max(k - 2, 0)], meta_ref.at[k], meta_send.at[k], meta_recv.at[k],
            "fs", above if k % 2 == 1 else below,
        )

    def gather_gu(q):
        return remote(
            sgu_ref, hgu_ref.at[:, tp_rows(cols_f), :], gu_send.at[q - 1], gu_recv.at[q - 1], "tp", lax.rem(tp + q, m)
        )

    def gather_sd(q):
        return remote(
            sd_ref, hd_ref.at[:, tp_rows(down_cols)], sd_send.at[q - 1], sd_recv.at[q - 1], "tp", lax.rem(tp + q, m)
        )

    def slice_gs(r):
        peer = lax.rem(z + r, n)
        return remote(
            hgu_ref.at[:, pl.ds(pl.multiple_of(peer * own_h, own_h), own_h), :],
            gs_ref.at[:, :, pl.ds(pl.multiple_of(z * deep, deep), deep)],
            gs_send.at[r - 1], gs_recv.at[r - 1], "fs", peer,
        )

    kinds = (
        (wg_ref, mg_ref, fg_ref), (wu_ref, mu_ref, fu_ref), (wd_ref, md_ref, fd_ref),
    )

    def mid_place(kind, first, count):
        if kind < 2:
            return (slice(None), slice(None), pl.ds(first * deep, count * deep))
        return (slice(None), pl.ds(first * down_rows, count * down_rows), slice(None))

    def weight_z(w, s, kind):
        peer = lax.rem(z + n - offset_of(s), n)
        src, mid, _ = kinds[kind]
        return remote(
            src.at[peer], mid.at[mid_place(kind, s, 1)], wz_send.at[w, kind], wz_recv.at[w, kind], "fs", peer
        )

    def weight_own(kind):
        src, mid, _ = kinds[kind]
        return pltpu.make_async_copy(src.at[z], mid.at[mid_place(kind, 0, 1)], wz_own.at[kind])

    def weight_group(w):
        return range(max(1, w * GROUP), (w + 1) * GROUP)

    def weight_z_all(w, kind):
        of = weight_group(w)
        src, mid, _ = kinds[kind]
        return remote(
            src.at[pl.ds(0, len(of))], mid.at[mid_place(kind, of[0], len(of))],
            wz_send.at[w, kind], wz_recv.at[w, kind], "fs", above,
        )

    def piece(w, kind, who):
        if kind < 2:
            return who, slice(None), pl.ds(w * GROUP * deep, GROUP * deep)
        return who, pl.ds(w * GROUP * down_rows, GROUP * down_rows), slice(None)

    def landing(w, kind, where):
        if kind < 2:
            return where, pl.ds(w * GROUP * deep, GROUP * deep)
        return pl.ds(w * GROUP * down_rows, GROUP * down_rows), where

    def weight_x(w, q, kind):
        peer = lax.rem(tp + q, m)
        _, mid, final = kinds[kind]
        where = tp_rows(cols_f if kind < 2 else down_cols)
        return remote(
            mid.at[piece(w, kind, peer)], final.at[landing(w, kind, where)],
            wx_send.at[w, kind], wx_recv.at[w, kind], "tp", peer,
        )

    def weight_x_all(w, kind):
        _, mid, final = kinds[kind]
        where = pl.ds(0, (m - 1) * (cols_f if kind < 2 else down_cols))
        return remote(
            mid.at[piece(w, kind, pl.ds(0, m - 1))], final.at[landing(w, kind, where)],
            wx_send.at[w, kind], wx_recv.at[w, kind], "tp", lax.rem(tp + 1, m),
        )

    def exchange(g, q):
        peer = lax.rem(tp + q, m)
        return remote(stage_ref.at[g, :, peer], x_ref.at[g, :, tp], x_send.at[g], x_recv.at[g], "tp", peer)

    def exchange_all(g):
        some = pl.ds(0, m - 1)
        return remote(
            stage_ref.at[g, :, some], x_ref.at[g, :, some], x_send.at[g], x_recv.at[g], "tp", lax.rem(tp + 1, m)
        )

    def answer(g, c, q):
        peer = lax.rem(tp + q, m)
        return remote(stage_ref.at[g, c, peer], rv_ref.at[g, c, tp], y_send.at[g, c], y_recv.at[g, c], "tp", peer)

    def answer_all(g, c):
        some = pl.ds(0, m - 1)
        return remote(
            stage_ref.at[g, c, some], rv_ref.at[g, c, some], y_send.at[g, c], y_recv.at[g, c], "tp", lax.rem(tp + 1, m)
        )

    for k in (1, 2):
        ring_meta(k).start()
        for p in range(AG_PIECES):
            ring(k, p).start()
    for kind in range(3):
        weight_own(kind).start()
    for q in range(1, m):
        gather_gu(q).start()
        gather_sd(q).start()
    for q in range(1, m):
        gather_gu(q).wait_recv()
    for r in range(1, n):
        slice_gs(r).start()
    gs_ref[:, :, pl.ds(pl.multiple_of(z * deep, deep), deep)] = hgu_ref[
        :, pl.ds(pl.multiple_of(z * own_h, own_h), own_h), :
    ]

    before = lax.broadcasted_iota(jnp.int32, (rows, rows), 0) < lax.broadcasted_iota(jnp.int32, (rows, rows), 1)
    before = before.astype(jnp.float32).astype(jnp.bfloat16)
    served = (lax.broadcasted_iota(jnp.int32, (m, rows), 0) + m * z).astype(jnp.float32)
    places = lax.broadcasted_iota(jnp.int32, (slots, rows), 0).astype(jnp.float32)

    def select(g):
        for b in range(GROUP):
            k = g * GROUP + b
            meta = meta_ref[k]
            chosen = jnp.zeros((m, rows), jnp.float32)
            weight = jnp.zeros((m, rows), jnp.float32)
            for j in range(picks):
                hit = meta[j : j + 1, :] == served
                chosen = chosen + hit.astype(jnp.float32)
                weight = weight + jnp.where(hit, meta[picks + j : picks + j + 1, :], 0.0)
            rank = jnp.dot(chosen.astype(jnp.bfloat16), before, preferred_element_type=jnp.float32)
            code = jnp.where(chosen > 0.0, rank, ABSENT)
            cw_ref[k, pl.ds(0, m), :] = code
            cw_ref[k, pl.ds(m, m), :] = weight
            for q in range(m):
                hot = (jnp.broadcast_to(code[q : q + 1, :], (slots, rows)) + float(cap * b)) == places
                pick_ref[pl.ds(q * slots, slots), pl.ds(b * rows, rows)] = hot.astype(jnp.float32).astype(jnp.bfloat16)

        @pl.loop(0, parts)
        def _(c):
            cols = pl.ds(pl.multiple_of(c * wide, wide), wide)
            taken = jnp.dot(
                pick_ref[...], all_ref[pl.ds(g * GROUP * rows, GROUP * rows), cols],
                preferred_element_type=jnp.float32,
            ).astype(jnp.bfloat16)
            stage_ref[g, c] = taken.reshape(m, slots, wide)
            x_ref[g, c, tp] = stage_ref[g, c, tp]

        for q in range(1, m):
            exchange(g, q).start()

    issue = {}
    for i, w in enumerate(reversed(range(groups))):
        issue.setdefault(max(1, min(n - 3, W_FIRST + W_EVERY * i)), []).append(w)
    for k in range(1, n):
        ring_meta(k).wait_recv()
        if k + 2 < n:
            ring_meta(k + 2).start()
        for p in range(AG_PIECES):
            ring(k, p).wait_recv()
            if k + 2 < n:
                ring(k + 2, p).start()
        for w in issue.get(k, ()):
            for s in reversed(weight_group(w)):
                for kind in range(3):
                    weight_z(w, s, kind).start()
        if k % GROUP == GROUP - 1:
            select(k // GROUP)

    for r in range(1, n):
        slice_gs(r).wait_recv()
    for g in range(groups):
        some = pl.ds(g * GROUP * rows, GROUP * rows)
        both = lax.dot_general(
            all_ref[some, :], gs_ref[...].reshape(2 * own_h, width), (((1,), (1,)), ((), ())),
            preferred_element_type=jnp.float32,
        )
        gate, upper = both[:, :own_h], both[:, own_h:]
        h_ref[some, :] = (gate / (1.0 + jnp.exp(-gate)) * upper).astype(jnp.bfloat16)

    for kind in range(3):
        weight_own(kind).wait()
    for w in reversed(range(groups)):
        for kind in range(3):
            weight_z_all(w, kind).wait_recv()
        for q in range(1, m):
            for kind in range(3):
                weight_x(w, q, kind).start()
        for kind, (_, mid, final) in enumerate(kinds):
            where = tp_rows(cols_f if kind < 2 else down_cols)
            final[landing(w, kind, where)] = mid[piece(w, kind, tp)]
    for w in reversed(range(groups)):
        for kind in range(3):
            weight_x_all(w, kind).wait_recv()
        for s in range(w * GROUP, (w + 1) * GROUP):
            source = lax.rem(z + n + offset_of(s), n)
            at = pl.ds(pl.multiple_of(source * deep, deep), deep)
            gate_ref[:, at] = fg_ref[:, pl.ds(s * deep, deep)]
            up_ref[:, at] = fu_ref[:, pl.ds(s * deep, deep)]
            down_ref[pl.ds(pl.multiple_of(source * down_rows, down_rows), down_rows), :] = fd_ref[
                pl.ds(s * down_rows, down_rows), :
            ]

    for g in range(groups):
        exchange_all(g).wait_send()
        exchange_all(g).wait_recv()

    def experts(first, count):
        @pl.loop(0, count)
        def _(i):
            g = first - i
            gate = jnp.zeros((lanes, gate_ref.shape[0]), jnp.float32)
            upper = jnp.zeros((lanes, gate_ref.shape[0]), jnp.float32)
            for c in range(parts):
                x = x_ref[g, c].reshape(lanes, wide)
                cols = pl.ds(c * wide, wide)
                nt = (((1,), (1,)), ((), ()))
                gate += lax.dot_general(x, gate_ref[:, cols], nt, preferred_element_type=jnp.float32)
                upper += lax.dot_general(x, up_ref[:, cols], nt, preferred_element_type=jnp.float32)
            hidden = (gate / (1.0 + jnp.exp(-gate)) * upper).astype(jnp.bfloat16)

            @pl.loop(0, parts)
            def _(c):
                cols = pl.ds(pl.multiple_of(c * wide, wide), wide)
                y = jnp.dot(hidden, down_ref[:, cols], preferred_element_type=jnp.float32)
                stage_ref[g, c] = y.astype(jnp.bfloat16).reshape(m, slots, wide)
                rv_ref[g, c, tp] = stage_ref[g, c, tp]
                for q in range(1, m):
                    answer(g, c, q).start()

    def spread(g):
        exact = jnp.transpose(cw_ref[pl.ds(g * GROUP, GROUP)].reshape(GROUP * 2 * m, rows))
        high = exact.astype(jnp.bfloat16)
        low = (exact - high.astype(jnp.float32)).astype(jnp.bfloat16)
        for b in range(GROUP):
            code = jnp.dot(high, ecode_ref[b], preferred_element_type=jnp.float32)
            hit = (code + float(cap * b)) == place_ref[...]
            for i, term in enumerate((high, low)):
                value = jnp.dot(term, ew_ref[b], preferred_element_type=jnp.float32)
                c_ref[pl.ds(b * rows, rows), pl.ds(i * lanes, lanes)] = jnp.where(hit, value, 0.0).astype(jnp.bfloat16)

    def combine(g, c):
        answer_all(g, c).wait_recv()
        some = pl.ds(g * GROUP * rows, GROUP * rows)
        cols = pl.ds(pl.multiple_of(c * wide, wide), wide)
        back = rv_ref[g, c].reshape(lanes, wide)
        total = jnp.dot(c_ref[:, pl.ds(0, lanes)], back, preferred_element_type=jnp.float32)
        total += jnp.dot(c_ref[:, pl.ds(lanes, lanes)], back, preferred_element_type=jnp.float32)
        total += jnp.dot(h_ref[some, :], hd_ref[:, cols], preferred_element_type=jnp.float32)
        d_ref[c] = total

    def share(offset, c):
        return d_ref[c, pl.ds((slot_of(offset) % GROUP) * rows, rows), :]

    def hop(sign, r, c):
        if sign > 0:
            return remote(pst_ref.at[r % 2, c], pin_ref.at[r - 1, c],
                          p_send.at[r - 1, c], p_recv.at[r - 1, c], "fs", above)
        return remote(mst_ref.at[r % 2, c], min_ref.at[r - 1, c],
                      m_send.at[r - 1, c], m_recv.at[r - 1, c], "fs", below)

    def forward(sign, r, c):
        last = half - 1 if sign > 0 else half
        total = share(sign * r, c)
        if r < last:
            hop(sign, r + 1, c).wait_recv()
            total = total + (pin_ref if sign > 0 else min_ref)[r, c].astype(jnp.float32)
        if r + 2 <= last:
            hop(sign, r + 2, c).wait_send()
        (pst_ref if sign > 0 else mst_ref)[r % 2, c] = total.astype(jnp.bfloat16)
        hop(sign, r, c).start()

    for q in range(1, m):
        gather_sd(q).wait_recv()
    early = min(2, groups)
    experts(groups - 1, early)
    spread(groups - 1)
    for i in range(half):
        g = groups - 1 - i // 2

        if i % 2 == 1 and g > 0:
            spread(g - 1)

        @pl.loop(0, parts)
        def _(c):
            if i == 0:
                combine(g, c)
            forward(-1, half - i, c)
            if half - 1 - i > 0:
                forward(1, half - 1 - i, c)
            if i % 2 == 1 and g > 0:
                combine(g - 1, c)

        if i == 0 and groups > early:
            experts(groups - 1 - early, groups - early)

    @pl.loop(0, parts)
    def _(c):
        hop(1, 1, c).wait_recv()
        hop(-1, 1, c).wait_recv()
        total = share(0, c) + pin_ref[0, c].astype(jnp.float32) + min_ref[0, c].astype(jnp.float32)
        out_ref[:, pl.ds(pl.multiple_of(c * wide, wide), wide)] = total.astype(jnp.bfloat16)

    for c in range(parts):
        for r in range(1, min(2, half - 1) + 1):
            hop(1, r, c).wait_send()
        for r in range(1, min(2, half) + 1):
            hop(-1, r, c).wait_send()
        for g in range(groups):
            answer_all(g, c).wait_send()
    for q in range(1, m):
        gather_gu(q).wait_send()
        gather_sd(q).wait_send()
    for r in range(1, n):
        slice_gs(r).wait_send()
    for k in range(1, n):
        ring_meta(k).wait_send()
        for p in range(AG_PIECES):
            ring(k, p).wait_send()
    for w in range(groups):
        for kind in range(3):
            weight_z_all(w, kind).wait_send()
            weight_x_all(w, kind).wait_send()


def on_device(
    tokens, route_ids, route_scores, norm_gain,
    expert_gate, expert_up, expert_down, shared_gate, shared_up, shared_down,
):
    n = lax.axis_size("fs")
    m = lax.axis_size("tp")
    experts = n * m
    rows, width = tokens.shape
    picks = route_ids.shape[1]
    cap = 3 * rows * picks // (2 * experts)
    slots = GROUP * cap
    lanes = m * slots
    groups = n // GROUP
    half = n // 2
    bf16, f32 = jnp.bfloat16, jnp.float32
    dma = pltpu.SemaphoreType.DMA
    wide = min(512, width)
    parts = width // wide

    deep, cols_f = expert_gate.shape[1:]
    down_rows, down_cols = expert_down.shape[1:]
    hidden = m * cols_f
    own_h = hidden // n

    def turned(weight):
        return (norm_gain[None, None, :] * jnp.swapaxes(weight, 1, 2)).astype(bf16).reshape(n, m, cols_f, deep)

    shared_t = jnp.stack([
        (norm_gain[None, :] * shared_gate.T).astype(bf16), (norm_gain[None, :] * shared_up.T).astype(bf16),
    ])
    lane = np.arange(lanes)
    row = np.arange(GROUP * 2 * m)
    block = np.arange(GROUP)

    def expand(first):
        wanted = block[:, None, None] * 2 * m + first + (lane // slots)[None, None, :]
        return jnp.asarray((row[None, :, None] == wanted).astype(np.float32), bf16)

    place = jnp.asarray((lane % slots)[None, :].astype(np.float32))
    held = pl.BlockSpec(memory_space=pl.ANY)
    mixed, gate_t, up_t, served_down, held_gu, held_down = pl.pallas_call(
        functools.partial(kernel, n, m, cap),
        out_shape=(
            jax.ShapeDtypeStruct((rows, width), bf16),
            jax.ShapeDtypeStruct((hidden, width), bf16),
            jax.ShapeDtypeStruct((hidden, width), bf16),
            jax.ShapeDtypeStruct((hidden, width), bf16),
            jax.ShapeDtypeStruct((2, hidden, deep), bf16),
            jax.ShapeDtypeStruct((down_rows, width), bf16),
        ),
        in_specs=[VMEM] * 5 + [held] * 3 + [VMEM] * 3,
        out_specs=(VMEM,) * 6,
        scratch_shapes=[
            pltpu.VMEM((n * rows, width), bf16),
            pltpu.VMEM((n, 2 * picks, rows), f32),
            pltpu.VMEM((n, 2 * m, rows), f32),
            pltpu.VMEM((groups, parts, m, slots, wide), bf16),
            pltpu.VMEM((groups, parts, m, slots, wide), bf16),
            pltpu.VMEM((groups, parts, m, slots, wide), bf16),
            pltpu.VMEM((lanes, GROUP * rows), bf16),
            pltpu.VMEM((2, own_h, width), bf16),
            pltpu.VMEM((n * rows, own_h), bf16),
            pltpu.VMEM((m, cols_f, width), bf16),
            pltpu.VMEM((m, cols_f, width), bf16),
            pltpu.VMEM((m, n * down_rows, down_cols), bf16),
            pltpu.VMEM((hidden, width), bf16),
            pltpu.VMEM((hidden, width), bf16),
            pltpu.VMEM((hidden, width), bf16),
            pltpu.VMEM((GROUP * rows, 2 * lanes), bf16),
            pltpu.VMEM((parts, GROUP * rows, wide), f32),
            pltpu.VMEM((half - 1, parts, rows, wide), bf16),
            pltpu.VMEM((half, parts, rows, wide), bf16),
            pltpu.VMEM((2, parts, rows, wide), bf16),
            pltpu.VMEM((2, parts, rows, wide), bf16),
            dma((n, AG_PIECES)), dma((n, AG_PIECES)), dma((n,)), dma((n,)),
            dma((groups,)), dma((groups,)), dma((groups, parts)), dma((groups, parts)),
            dma((m - 1,)), dma((m - 1,)), dma((m - 1,)), dma((m - 1,)), dma((n - 1,)), dma((n - 1,)),
            dma((groups, 3)), dma((groups, 3)), dma((3,)), dma((groups, 3)), dma((groups, 3)),
            dma((half - 1, parts)), dma((half - 1, parts)), dma((half, parts)), dma((half, parts)),
        ],
        compiler_params=pltpu.CompilerParams(
            collective_id=0, has_side_effects=True, vmem_limit_bytes=63 * 1024 * 1024,
        ),
        cost_estimate=pl.CostEstimate(flops=100_000_000_000, bytes_accessed=30_000_000, transcendentals=0),
        name="hand_over",
    )(
        tokens, route_ids.T, route_scores.T, shared_t, shared_down.astype(bf16),
        turned(expert_gate), turned(expert_up), expert_down.astype(bf16).reshape(n, m, down_rows, down_cols),
        expand(0), expand(m), place,
    )
    return (mixed, gate_t.T[None], up_t.T[None], served_down[None], held_gu[0].T, held_gu[1].T, held_down)


def solution(mesh):
    return jax.shard_map(
        on_device,
        mesh=mesh,
        in_specs=(
            P(("grp", "fs", "tp"), None),
            P(("grp", "fs", "tp"), None),
            P(("grp", "fs", "tp"), None),
            P("fs"),
            P(None, "fs", "tp"),
            P(None, "fs", "tp"),
            P(None, "fs", "tp"),
            P("fs", "tp"),
            P("fs", "tp"),
            P("fs", "tp"),
        ),
        out_specs=(
            P(("grp", "fs", "tp"), None),
            P(("grp", "fs", "tp"), None, None),
            P(("grp", "fs", "tp"), None, None),
            P(("grp", "fs", "tp"), None, None),
            P(("grp", "fs"), None),
            P(("grp", "fs"), None),
            P(("grp", "fs"), None),
        ),
        check_vma=False,
    )
```

time: 453 us -> 423 us (0.934)
  starting transfers between devices: 31.2 us -> 0 us
  local copies, waits for them, and re-layouts: 26.6 us -> 7.6 us
  Pallas kernels: 388 us -> 405 us
    all_to_all x1 -> x0, starting transfers between devices: 31.2 us -> none  [on_device(): lax.all_to_all(packed, ('fs', 'tp'), split_axis=0, concat_axis=0, tiled=T...]
    pallas_call x2 -> x1, Pallas kernels: 388 us -> 405 us  [on_device(): pl.pallas_call(functools.partial(kernel, n, m, cap), out_shape=(jax.Shape...]
    reshape x4 -> x0, local copies, waits for them, and re-layouts: 5.51 us -> none  [the longest x2 3.56 us: served(): return jnp.transpose(tile, (0, 3, 1, 2)).reshape(n * deep, m * cols_f)]
    transpose x5 -> x0, local copies, waits for them, and re-layouts: 5.09 us -> none  [the longest x2 2.58 us: served(): return jnp.transpose(tile, (0, 3, 1, 2)).reshape(n * deep, m * cols_f)]
    unnamed x32 -> x21, local copies, waits for them, and re-layouts: 9.89 us -> 7.59 us
  transfers between devices with their start and end apart: 1 -> 0, of which waited for: 0 -> 0; matrix products, arithmetic and copies ran while one was open for 1% -> 0% of each run, Pallas kernels for 58% -> 0%
where the time goes in v2:
time: 423 us
  Pallas kernels  405 us (96%)
  other arithmetic  8.95 us (2%)
  local copies, waits for them, and re-layouts  7.6 us (2%)
    pallas_call x1, Pallas kernels, on_device(): pl.pallas_call(functools.partial(kernel, n, m, cap), out_shape=(jax.Shape...  405 us

profile of v2, /device:TPU:33, one launch (start us, length us, event | category | flops | bytes accessed | tf_op | source)
XLA Modules:
  0.0 422.7 jit_solution(2896357019595688794)
XLA Ops:
  0.6 0.0 copy-start.6
  0.6 0.0 copy-start
  0.7 1.5 convert_element_type.34.sd_ref
  2.1 0.8 fusion
  2.9 0.6 pad_maximum_fusion.sgu_ref
  3.5 2.7 convert_element_type.39
  6.2 0.0 copy-done.6
  6.2 0.0 copy-done
  6.2 3.4 multiply_convert_fusion
  9.6 405.4 %hand_over.1 = (bf16[128,2048]{1,0:T(8,128)(2,1)}, bf16[256,2048]{1,0:T(8,128)(2,1)}, bf16[256,2048]{1,0:T(8,128)(2,1)}, bf16[256,2048]{1,0:T(8,128)(2,1)}, bf16...) custom-call(bf16[128,2048]{1,0:T(8,128)(2,1)} %tok_ref.1, s32[8,128]{1,0:T(8,128)} %bitcast.38, f32[8,128]{1,0:T(8,128)} %bitcast.39, ...), custom_call_target="tpu_custom_call" | custom-call | flops 99999997952 | bytes 30000000 | tf_op jit(solution)/shard_map/hand_over/pallas_call | solution.py:463
  415.1 0.0 copy-start.4
  415.1 0.0 copy-start.2
  415.1 0.0 copy-start.3
  415.1 2.4 copy.20
  417.5 0.0 copy-done.4
  417.5 0.0 copy-start.1
  417.5 0.7 copy.23
  418.2 0.7 copy.22
  419.0 0.0 copy-done.2
  419.0 1.3 copy.21
  420.3 0.0 copy-done.3
  420.3 0.0 copy-start.5
  420.3 0.8 copy.27
  421.1 0.0 copy-done.1
  421.1 1.0 copy.28
  422.0 0.0 copy-done.5
  422.0 0.6 copy.29
  (1 shorter events, 0.0 us)
Async XLA Ops:
  0.6 5.6 %copy-start.6 = (f32[128]{0:T(128)S(1)}, f32[128]{0:T(128)}, u32[]{:S(2)}) copy-start(f32[128]{0:T(128)} %param.16) | copy-start | bytes 1540
  0.6 5.5 %copy-start = (f32[128,128,32]{1,2,0:T(8,128)S(1)}, f32[128,128,32]{1,2,0:T(8,128)}, u32[]{:S(2)}) copy-start(f32[128,128,32]{1,2,0:T(8,128)} %param.18) | copy-start | bytes 6291460
  415.1 2.4 copy-start.4
  415.1 3.9 copy-start.2
  415.1 5.2 %copy-start.3 = (bf16[128,2048]{1,0:T(8,128)(2,1)S(1)}, bf16[128,2048]{1,0:T(8,128)(2,1)}, u32[]{:S(2)}) copy-start(bf16[128,2048]{1,0:T(8,128)(2,1)} %get-tuple-element.39) | copy-start | bytes 1572868
  417.5 3.6 copy-start.1
  420.3 1.8 copy-start.5

commit v3 on v2

--- a/solution.py
+++ b/solution.py
@@ -14,7 +14,7 @@
 MESH = pl.DeviceIdType.MESH
 GROUP = 4
 AG_PIECES = 2
-W_FIRST, W_EVERY = 5, 4
+LOADS = 4
 VMEM = pl.BlockSpec(memory_space=pltpu.VMEM)
 
 
@@ -46,24 +46,37 @@
     return slot // 2 if slot % 2 == 0 else -((slot + 1) // 2)
 
 
+def weight_order(n):
+    order, far, near = [0, n - 1], n - 2, 1
+    while near <= far:
+        order.append(far)
+        if near < far:
+            order.append(near)
+        far, near = far - 1, near + 1
+    return order
+
+
 def kernel(
-    n, m, cap, tok_ref, ids_ref, sc_ref, sgu_ref, sd_ref, wg_ref, wu_ref, wd_ref, ecode_ref, ew_ref, place_ref,
+    n, m, cap, tok_ref, ids_ref, sc_ref, gain_ref, sg_ref, su_ref, sd32_ref, eg_ref, eu_ref, ed_ref,
+    ecode_ref, ew_ref, place_ref,
     out_ref, gate_ref, up_ref, down_ref, hgu_ref, hd_ref,
-    all_ref, meta_ref, cw_ref, stage_ref, x_ref, rv_ref, pick_ref, gs_ref, h_ref,
+    all_ref, meta_ref, cw_ref, stage_ref, x_ref, rv_ref, pick_ref, gs_ref,
+    sgu_ref, sd_ref, eg32_ref, eu32_ref, ed32_ref, wg_ref, wu_ref, wd_ref,
     mg_ref, mu_ref, md_ref, fg_ref, fu_ref, fd_ref, c_ref, d_ref, pin_ref, min_ref, pst_ref, mst_ref,
     ag_send, ag_recv, meta_send, meta_recv, x_send, x_recv, y_send, y_recv,
     gu_send, gu_recv, sd_send, sd_recv, gs_send, gs_recv,
-    wz_send, wz_recv, wz_own, wx_send, wx_recv, p_send, p_recv, m_send, m_recv,
+    load_sem, wz_send, wz_recv, wx_send, wx_recv, p_send, p_recv, m_send, m_recv,
 ):
     z, tp = lax.axis_index("fs"), lax.axis_index("tp")
     rows, width = tok_ref.shape
     picks = ids_ref.shape[0]
     above, below = lax.rem(z + 1, n), lax.rem(z + n - 1, n)
-    parts, wide = stage_ref.shape[1], stage_ref.shape[4]
+    parts, wide = stage_ref.shape[1], stage_ref.shape[3]
     slots = GROUP * cap
     lanes = m * slots
     half, groups = n // 2, n // GROUP
     cols_f, deep = sgu_ref.shape[1:]
+    order = weight_order(n)
     own_h = gs_ref.shape[1]
     down_rows, down_cols = sd_ref.shape
 
@@ -77,6 +90,10 @@
     scores = sc_ref[...]
     meta_ref[0, pl.ds(0, picks), :] = ids_ref[...].astype(jnp.float32)
     meta_ref[0, pl.ds(picks, picks), :] = route_scale * scores / jnp.sum(scores, axis=0, keepdims=True)
+    gain = gain_ref[...]
+    sgu_ref[0] = (gain * sg_ref[...]).astype(jnp.bfloat16)
+    sgu_ref[1] = (gain * su_ref[...]).astype(jnp.bfloat16)
+    sd_ref[...] = sd32_ref[...].astype(jnp.bfloat16)
     hgu_ref[:, tp_rows(cols_f), :] = sgu_ref[...]
     hd_ref[:, tp_rows(down_cols)] = sd_ref[...]
     pl.semaphore_wait(barrier, arrivals)
@@ -124,25 +141,20 @@
             return (slice(None), slice(None), pl.ds(first * deep, count * deep))
         return (slice(None), pl.ds(first * down_rows, count * down_rows), slice(None))
 
-    def weight_z(w, s, kind):
-        peer = lax.rem(z + n - offset_of(s), n)
+    def weight_z(at, kind):
+        peer = lax.rem(z + n - offset_of(order[at]), n)
         src, mid, _ = kinds[kind]
-        return remote(
-            src.at[peer], mid.at[mid_place(kind, s, 1)], wz_send.at[w, kind], wz_recv.at[w, kind], "fs", peer
-        )
-
-    def weight_own(kind):
-        src, mid, _ = kinds[kind]
-        return pltpu.make_async_copy(src.at[z], mid.at[mid_place(kind, 0, 1)], wz_own.at[kind])
-
-    def weight_group(w):
-        return range(max(1, w * GROUP), (w + 1) * GROUP)
+        w = at // GROUP
+        return remote(
+            src.at[peer], mid.at[mid_place(kind, at, 1)], wz_send.at[w, kind], wz_recv.at[w, kind], "fs", peer
+        )
 
     def weight_z_all(w, kind):
-        of = weight_group(w)
-        src, mid, _ = kinds[kind]
-        return remote(
-            src.at[pl.ds(0, len(of))], mid.at[mid_place(kind, of[0], len(of))],
+        first = max(1, w * GROUP)
+        count = (w + 1) * GROUP - first
+        _, mid, _ = kinds[kind]
+        return remote(
+            mid.at[mid_place(kind, first, count)], mid.at[mid_place(kind, first, count)],
             wz_send.at[w, kind], wz_recv.at[w, kind], "fs", above,
         )
 
@@ -166,42 +178,65 @@
         )
 
     def weight_x_all(w, kind):
-        _, mid, final = kinds[kind]
+        _, _, final = kinds[kind]
         where = pl.ds(0, (m - 1) * (cols_f if kind < 2 else down_cols))
         return remote(
-            mid.at[piece(w, kind, pl.ds(0, m - 1))], final.at[landing(w, kind, where)],
+            final.at[landing(w, kind, where)], final.at[landing(w, kind, where)],
             wx_send.at[w, kind], wx_recv.at[w, kind], "tp", lax.rem(tp + 1, m),
         )
+
+    def of(who):
+        return pl.ds(pl.multiple_of(who * slots, slots), slots)
+
+    most = pl.ds(0, (m - 1) * slots)
 
     def exchange(g, q):
         peer = lax.rem(tp + q, m)
-        return remote(stage_ref.at[g, :, peer], x_ref.at[g, :, tp], x_send.at[g], x_recv.at[g], "tp", peer)
+        return remote(stage_ref.at[g, :, of(peer)], x_ref.at[g, :, of(tp)], x_send.at[g], x_recv.at[g], "tp", peer)
 
     def exchange_all(g):
-        some = pl.ds(0, m - 1)
-        return remote(
-            stage_ref.at[g, :, some], x_ref.at[g, :, some], x_send.at[g], x_recv.at[g], "tp", lax.rem(tp + 1, m)
+        return remote(
+            stage_ref.at[g, :, most], x_ref.at[g, :, most], x_send.at[g], x_recv.at[g], "tp", lax.rem(tp + 1, m)
         )
 
     def answer(g, c, q):
         peer = lax.rem(tp + q, m)
-        return remote(stage_ref.at[g, c, peer], rv_ref.at[g, c, tp], y_send.at[g, c], y_recv.at[g, c], "tp", peer)
+        return remote(
+            stage_ref.at[g, c, of(peer)], rv_ref.at[g, c, of(tp)], y_send.at[g, c], y_recv.at[g, c], "tp", peer
+        )
 
     def answer_all(g, c):
-        some = pl.ds(0, m - 1)
-        return remote(
-            stage_ref.at[g, c, some], rv_ref.at[g, c, some], y_send.at[g, c], y_recv.at[g, c], "tp", lax.rem(tp + 1, m)
-        )
-
+        return remote(
+            stage_ref.at[g, c, most], rv_ref.at[g, c, most], y_send.at[g, c], y_recv.at[g, c], "tp", lax.rem(tp + 1, m)
+        )
+
+    span = n // LOADS
+    loads = ((eg_ref, eg32_ref), (eu_ref, eu32_ref), (ed_ref, ed32_ref))
+
+    def load(i, kind):
+        src, dst = loads[kind]
+        return pltpu.make_async_copy(src.at[pl.ds(i * span, span)], dst.at[i % 2], load_sem.at[i % 2, kind])
+
+    for kind in range(3):
+        load(0, kind).start()
     for k in (1, 2):
         ring_meta(k).start()
         for p in range(AG_PIECES):
             ring(k, p).start()
-    for kind in range(3):
-        weight_own(kind).start()
     for q in range(1, m):
         gather_gu(q).start()
         gather_sd(q).start()
+    for i in range(LOADS):
+        for kind in range(3):
+            if i + 1 < LOADS:
+                load(i + 1, kind).start()
+            load(i, kind).wait()
+        some = pl.ds(i * span, span)
+        wg_ref[some] = (gain * eg32_ref[i % 2]).astype(jnp.bfloat16)
+        wu_ref[some] = (gain * eu32_ref[i % 2]).astype(jnp.bfloat16)
+        wd_ref[some] = ed32_ref[i % 2].astype(jnp.bfloat16)
+    for kind, (src, mid, _) in enumerate(kinds):
+        mid[mid_place(kind, 0, 1)] = src[z]
     for q in range(1, m):
         gather_gu(q).wait_recv()
     for r in range(1, n):
@@ -240,15 +275,28 @@
                 pick_ref[...], all_ref[pl.ds(g * GROUP * rows, GROUP * rows), cols],
                 preferred_element_type=jnp.float32,
             ).astype(jnp.bfloat16)
-            stage_ref[g, c] = taken.reshape(m, slots, wide)
-            x_ref[g, c, tp] = stage_ref[g, c, tp]
+            stage_ref[g, c] = taken
+            x_ref[g, c, of(tp), :] = stage_ref[g, c, of(tp), :]
 
         for q in range(1, m):
             exchange(g, q).start()
 
+    moved_on = []
+
+    def move_on(w):
+        moved_on.append(w)
+        for kind in range(3):
+            weight_z_all(w, kind).wait_recv()
+        for q in range(1, m):
+            for kind in range(3):
+                weight_x(w, q, kind).start()
+        for kind, (_, mid, final) in enumerate(kinds):
+            where = tp_rows(cols_f if kind < 2 else down_cols)
+            final[landing(w, kind, where)] = mid[piece(w, kind, tp)]
+
     issue = {}
-    for i, w in enumerate(reversed(range(groups))):
-        issue.setdefault(max(1, min(n - 3, W_FIRST + W_EVERY * i)), []).append(w)
+    for at in range(1, n):
+        issue.setdefault(max(1, min(n - 3, 1 + 2 * (at // 2))), []).append(at)
     for k in range(1, n):
         ring_meta(k).wait_recv()
         if k + 2 < n:
@@ -257,12 +305,13 @@
             ring(k, p).wait_recv()
             if k + 2 < n:
                 ring(k + 2, p).start()
-        for w in issue.get(k, ()):
-            for s in reversed(weight_group(w)):
-                for kind in range(3):
-                    weight_z(w, s, kind).start()
+        for at in issue.get(k, ()):
+            for kind in range(3):
+                weight_z(at, kind).start()
         if k % GROUP == GROUP - 1:
             select(k // GROUP)
+            if groups > 2 and k // GROUP >= groups - 2:
+                move_on(k // GROUP - groups + 2)
 
     for r in range(1, n):
         slice_gs(r).wait_recv()
@@ -273,29 +322,32 @@
             preferred_element_type=jnp.float32,
         )
         gate, upper = both[:, :own_h], both[:, own_h:]
-        h_ref[some, :] = (gate / (1.0 + jnp.exp(-gate)) * upper).astype(jnp.bfloat16)
-
-    for kind in range(3):
-        weight_own(kind).wait()
-    for w in reversed(range(groups)):
-        for kind in range(3):
-            weight_z_all(w, kind).wait_recv()
-        for q in range(1, m):
-            for kind in range(3):
-                weight_x(w, q, kind).start()
-        for kind, (_, mid, final) in enumerate(kinds):
-            where = tp_rows(cols_f if kind < 2 else down_cols)
-            final[landing(w, kind, where)] = mid[piece(w, kind, tp)]
-    for w in reversed(range(groups)):
+        c_ref[g, :, pl.ds(lanes, own_h)] = (gate / (1.0 + jnp.exp(-gate)) * upper).astype(jnp.bfloat16)
+        turned = jnp.transpose(cw_ref[pl.ds(g * GROUP, GROUP)].reshape(GROUP * 2 * m, rows)).astype(jnp.bfloat16)
+        for b in range(GROUP):
+            code = jnp.dot(turned, ecode_ref[b], preferred_element_type=jnp.float32)
+            value = jnp.dot(turned, ew_ref[b], preferred_element_type=jnp.float32)
+            hit = (code + float(cap * b)) == place_ref[...]
+            c_ref[g, pl.ds(b * rows, rows), pl.ds(0, lanes)] = jnp.where(hit, value, 0.0).astype(jnp.bfloat16)
+    for q in range(1, m):
+        gather_sd(q).wait_recv()
+    for g in range(groups):
+        for c in range(parts):
+            rv_ref[g, c, pl.ds(lanes, own_h), :] = hd_ref[:, pl.ds(c * wide, wide)]
+
+    for w in range(groups):
+        if w not in moved_on:
+            move_on(w)
+    for w in range(groups):
         for kind in range(3):
             weight_x_all(w, kind).wait_recv()
-        for s in range(w * GROUP, (w + 1) * GROUP):
-            source = lax.rem(z + n + offset_of(s), n)
-            at = pl.ds(pl.multiple_of(source * deep, deep), deep)
-            gate_ref[:, at] = fg_ref[:, pl.ds(s * deep, deep)]
-            up_ref[:, at] = fu_ref[:, pl.ds(s * deep, deep)]
+        for at in range(w * GROUP, (w + 1) * GROUP):
+            source = lax.rem(z + n + offset_of(order[at]), n)
+            there = pl.ds(pl.multiple_of(source * deep, deep), deep)
+            gate_ref[:, there] = fg_ref[:, pl.ds(at * deep, deep)]
+            up_ref[:, there] = fu_ref[:, pl.ds(at * deep, deep)]
             down_ref[pl.ds(pl.multiple_of(source * down_rows, down_rows), down_rows), :] = fd_ref[
-                pl.ds(s * down_rows, down_rows), :
+                pl.ds(at * down_rows, down_rows), :
             ]
 
     for g in range(groups):
@@ -309,7 +361,7 @@
             gate = jnp.zeros((lanes, gate_ref.shape[0]), jnp.float32)
             upper = jnp.zeros((lanes, gate_ref.shape[0]), jnp.float32)
             for c in range(parts):
-                x = x_ref[g, c].reshape(lanes, wide)
+                x = x_ref[g, c]
                 cols = pl.ds(c * wide, wide)
                 nt = (((1,), (1,)), ((), ()))
                 gate += lax.dot_general(x, gate_ref[:, cols], nt, preferred_element_type=jnp.float32)
@@ -320,31 +372,14 @@
             def _(c):
                 cols = pl.ds(pl.multiple_of(c * wide, wide), wide)
                 y = jnp.dot(hidden, down_ref[:, cols], preferred_element_type=jnp.float32)
-                stage_ref[g, c] = y.astype(jnp.bfloat16).reshape(m, slots, wide)
-                rv_ref[g, c, tp] = stage_ref[g, c, tp]
+                stage_ref[g, c] = y.astype(jnp.bfloat16)
+                rv_ref[g, c, of(tp), :] = stage_ref[g, c, of(tp), :]
                 for q in range(1, m):
                     answer(g, c, q).start()
 
-    def spread(g):
-        exact = jnp.transpose(cw_ref[pl.ds(g * GROUP, GROUP)].reshape(GROUP * 2 * m, rows))
-        high = exact.astype(jnp.bfloat16)
-        low = (exact - high.astype(jnp.float32)).astype(jnp.bfloat16)
-        for b in range(GROUP):
-            code = jnp.dot(high, ecode_ref[b], preferred_element_type=jnp.float32)
-            hit = (code + float(cap * b)) == place_ref[...]
-            for i, term in enumerate((high, low)):
-                value = jnp.dot(term, ew_ref[b], preferred_element_type=jnp.float32)
-                c_ref[pl.ds(b * rows, rows), pl.ds(i * lanes, lanes)] = jnp.where(hit, value, 0.0).astype(jnp.bfloat16)
-
     def combine(g, c):
         answer_all(g, c).wait_recv()
-        some = pl.ds(g * GROUP * rows, GROUP * rows)
-        cols = pl.ds(pl.multiple_of(c * wide, wide), wide)
-        back = rv_ref[g, c].reshape(lanes, wide)
-        total = jnp.dot(c_ref[:, pl.ds(0, lanes)], back, preferred_element_type=jnp.float32)
-        total += jnp.dot(c_ref[:, pl.ds(lanes, lanes)], back, preferred_element_type=jnp.float32)
-        total += jnp.dot(h_ref[some, :], hd_ref[:, cols], preferred_element_type=jnp.float32)
-        d_ref[c] = total
+        d_ref[c] = jnp.dot(c_ref[g], rv_ref[g, c], preferred_element_type=jnp.float32)
 
     def share(offset, c):
         return d_ref[c, pl.ds((slot_of(offset) % GROUP) * rows, rows), :]
@@ -367,16 +402,10 @@
         (pst_ref if sign > 0 else mst_ref)[r % 2, c] = total.astype(jnp.bfloat16)
         hop(sign, r, c).start()
 
-    for q in range(1, m):
-        gather_sd(q).wait_recv()
     early = min(2, groups)
     experts(groups - 1, early)
-    spread(groups - 1)
     for i in range(half):
         g = groups - 1 - i // 2
-
-        if i % 2 == 1 and g > 0:
-            spread(g - 1)
 
         @pl.loop(0, parts)
         def _(c):
@@ -445,11 +474,8 @@
     own_h = hidden // n
 
     def turned(weight):
-        return (norm_gain[None, None, :] * jnp.swapaxes(weight, 1, 2)).astype(bf16).reshape(n, m, cols_f, deep)
-
-    shared_t = jnp.stack([
-        (norm_gain[None, :] * shared_gate.T).astype(bf16), (norm_gain[None, :] * shared_up.T).astype(bf16),
-    ])
+        return jnp.swapaxes(weight, 1, 2).reshape(n, m, cols_f, deep)
+
     lane = np.arange(lanes)
     row = np.arange(GROUP * 2 * m)
     block = np.arange(GROUP)
@@ -470,25 +496,32 @@
             jax.ShapeDtypeStruct((2, hidden, deep), bf16),
             jax.ShapeDtypeStruct((down_rows, width), bf16),
         ),
-        in_specs=[VMEM] * 5 + [held] * 3 + [VMEM] * 3,
+        in_specs=[VMEM] * 7 + [held] * 3 + [VMEM] * 3,
         out_specs=(VMEM,) * 6,
         scratch_shapes=[
             pltpu.VMEM((n * rows, width), bf16),
             pltpu.VMEM((n, 2 * picks, rows), f32),
             pltpu.VMEM((n, 2 * m, rows), f32),
-            pltpu.VMEM((groups, parts, m, slots, wide), bf16),
-            pltpu.VMEM((groups, parts, m, slots, wide), bf16),
-            pltpu.VMEM((groups, parts, m, slots, wide), bf16),
+            pltpu.VMEM((groups, parts, lanes, wide), bf16),
+            pltpu.VMEM((groups, parts, lanes, wide), bf16),
+            pltpu.VMEM((groups, parts, lanes + own_h, wide), bf16),
             pltpu.VMEM((lanes, GROUP * rows), bf16),
             pltpu.VMEM((2, own_h, width), bf16),
-            pltpu.VMEM((n * rows, own_h), bf16),
+            pltpu.VMEM((2, cols_f, deep), bf16),
+            pltpu.VMEM((down_rows, down_cols), bf16),
+            pltpu.VMEM((2, n // LOADS, m, cols_f, deep), f32),
+            pltpu.VMEM((2, n // LOADS, m, cols_f, deep), f32),
+            pltpu.VMEM((2, n // LOADS, m, down_rows, down_cols), f32),
+            pltpu.VMEM((n, m, cols_f, deep), bf16),
+            pltpu.VMEM((n, m, cols_f, deep), bf16),
+            pltpu.VMEM((n, m, down_rows, down_cols), bf16),
             pltpu.VMEM((m, cols_f, width), bf16),
             pltpu.VMEM((m, cols_f, width), bf16),
             pltpu.VMEM((m, n * down_rows, down_cols), bf16),
             pltpu.VMEM((hidden, width), bf16),
             pltpu.VMEM((hidden, width), bf16),
             pltpu.VMEM((hidden, width), bf16),
-            pltpu.VMEM((GROUP * rows, 2 * lanes), bf16),
+            pltpu.VMEM((groups, GROUP * rows, lanes + own_h), bf16),
             pltpu.VMEM((parts, GROUP * rows, wide), f32),
             pltpu.VMEM((half - 1, parts, rows, wide), bf16),
             pltpu.VMEM((half, parts, rows, wide), bf16),
@@ -497,7 +530,7 @@
             dma((n, AG_PIECES)), dma((n, AG_PIECES)), dma((n,)), dma((n,)),
             dma((groups,)), dma((groups,)), dma((groups, parts)), dma((groups, parts)),
             dma((m - 1,)), dma((m - 1,)), dma((m - 1,)), dma((m - 1,)), dma((n - 1,)), dma((n - 1,)),
-            dma((groups, 3)), dma((groups, 3)), dma((3,)), dma((groups, 3)), dma((groups, 3)),
+            dma((2, 3)), dma((groups, 3)), dma((groups, 3)), dma((groups, 3)), dma((groups, 3)),
             dma((half - 1, parts)), dma((half - 1, parts)), dma((half, parts)), dma((half, parts)),
         ],
         compiler_params=pltpu.CompilerParams(
@@ -506,8 +539,8 @@
         cost_estimate=pl.CostEstimate(flops=100_000_000_000, bytes_accessed=30_000_000, transcendentals=0),
         name="hand_over",
     )(
-        tokens, route_ids.T, route_scores.T, shared_t, shared_down.astype(bf16),
-        turned(expert_gate), turned(expert_up), expert_down.astype(bf16).reshape(n, m, down_rows, down_cols),
+        tokens, route_ids.T, route_scores.T, norm_gain[None, :], shared_gate.T, shared_up.T, shared_down,
+        turned(expert_gate), turned(expert_up), expert_down.reshape(n, m, down_rows, down_cols),
         expand(0), expand(m), place,
     )
     return (mixed, gate_t.T[None], up_t.T[None], served_down[None], held_gu[0].T, held_gu[1].T, held_down)

time: 423 us -> 392 us (0.927)
  Pallas kernels: 405 us -> 384 us
  other arithmetic: 8.95 us -> 0 us
    pallas_call x1, Pallas kernels: 405 us -> 384 us  [on_device(): pl.pallas_call(functools.partial(kernel, n, m, cap), out_shape=(jax.Shape...]
    convert_element_type x3 -> x0, other arithmetic: 7.58 us -> none  [the longest x1 3.42 us: turned(): (norm_gain[None, None, :] * jnp.swapaxes(weight, 1, 2)).astype(bf16)]
where the time goes in v3:
time: 392 us
  Pallas kernels  384 us (98%)
  local copies, waits for them, and re-layouts  7.59 us (2%)
    pallas_call x1, Pallas kernels, on_device(): pl.pallas_call(functools.partial(kernel, n, m, cap), out_shape=(jax.Shape...  384 us

profile of v3, /device:TPU:33, one launch (start us, length us, event | category | flops | bytes accessed | tf_op | source)
XLA Modules:
  0.0 392.0 jit_solution(153678140463553815)
XLA Ops:
  0.6 383.7 %hand_over.1 = (bf16[128,2048]{1,0:T(8,128)(2,1)}, bf16[256,2048]{1,0:T(8,128)(2,1)}, bf16[256,2048]{1,0:T(8,128)(2,1)}, bf16[256,2048]{1,0:T(8,128)(2,1)}, bf16...) custom-call(bf16[128,2048]{1,0:T(8,128)(2,1)} %tok_ref.1, s32[8,128]{1,0:T(8,128)} %bitcast.35, f32[8,128]{1,0:T(8,128)} %bitcast.36, ...), custom_call_target="tpu_custom_call" | custom-call | flops 99999997952 | bytes 30000000 | tf_op jit(solution)/shard_map/hand_over/pallas_call | solution.py:489
  384.4 0.0 copy-start.3
  384.4 0.0 copy-start.1
  384.4 0.0 copy-start.2
  384.4 2.4 copy.20
  386.8 0.0 copy-done.3
  386.8 0.0 copy-start
  386.8 0.7 copy.23
  387.6 0.7 copy.22
  388.3 0.0 copy-done.1
  388.3 1.3 copy.21
  389.6 0.0 copy-done.2
  389.6 0.0 copy-start.4
  389.6 0.8 copy.27
  390.4 0.0 copy-done
  390.4 1.0 copy.28
  391.4 0.0 copy-done.4
  391.4 0.6 copy.29
  (1 shorter events, 0.0 us)
Async XLA Ops:
  384.4 2.4 copy-start.3
  384.4 3.9 copy-start.1
  384.4 5.2 %copy-start.2 = (bf16[128,2048]{1,0:T(8,128)(2,1)S(1)}, bf16[128,2048]{1,0:T(8,128)(2,1)}, u32[]{:S(2)}) copy-start(bf16[128,2048]{1,0:T(8,128)(2,1)} %get-tuple-element.35) | copy-start | bytes 1572868
  386.8 3.6 copy-start
  389.6 1.8 copy-start.4

commit v4 on v3

--- a/solution.py
+++ b/solution.py
@@ -77,6 +77,8 @@
     half, groups = n // 2, n // GROUP
     cols_f, deep = sgu_ref.shape[1:]
     order = weight_order(n)
+    bundles = [(first, GROUP) for first in range(0, n - GROUP, GROUP)] + [(n - GROUP, GROUP - 1), (n - 1, 1)]
+    bundle_of = [w for w, (_, count) in enumerate(bundles) for _ in range(count)]
     own_h = gs_ref.shape[1]
     down_rows, down_cols = sd_ref.shape
 
@@ -102,10 +104,13 @@
 
     def ring(k, p):
         src = max(k - 2, 0)
+        upward = k % 2 == 1
+        if k == n - 1 and p >= AG_PIECES // 2:
+            src, upward = k - 1, False
         return remote(
             all_ref.at[pl.ds(src * rows + p * step_rows, step_rows), :],
             all_ref.at[pl.ds(k * rows + p * step_rows, step_rows), :],
-            ag_send.at[k, p], ag_recv.at[k, p], "fs", above if k % 2 == 1 else below,
+            ag_send.at[k, p], ag_recv.at[k, p], "fs", above if upward else below,
         )
 
     def ring_meta(k):
@@ -144,14 +149,14 @@
     def weight_z(at, kind):
         peer = lax.rem(z + n - offset_of(order[at]), n)
         src, mid, _ = kinds[kind]
-        w = at // GROUP
+        w = bundle_of[at]
         return remote(
             src.at[peer], mid.at[mid_place(kind, at, 1)], wz_send.at[w, kind], wz_recv.at[w, kind], "fs", peer
         )
 
     def weight_z_all(w, kind):
-        first = max(1, w * GROUP)
-        count = (w + 1) * GROUP - first
+        first, count = bundles[w]
+        first, count = max(1, first), count - (first == 0)
         _, mid, _ = kinds[kind]
         return remote(
             mid.at[mid_place(kind, first, count)], mid.at[mid_place(kind, first, count)],
@@ -159,14 +164,16 @@
         )
 
     def piece(w, kind, who):
+        first, count = bundles[w]
         if kind < 2:
-            return who, slice(None), pl.ds(w * GROUP * deep, GROUP * deep)
-        return who, pl.ds(w * GROUP * down_rows, GROUP * down_rows), slice(None)
+            return who, slice(None), pl.ds(first * deep, count * deep)
+        return who, pl.ds(first * down_rows, count * down_rows), slice(None)
 
     def landing(w, kind, where):
+        first, count = bundles[w]
         if kind < 2:
-            return where, pl.ds(w * GROUP * deep, GROUP * deep)
-        return pl.ds(w * GROUP * down_rows, GROUP * down_rows), where
+            return where, pl.ds(first * deep, count * deep)
+        return pl.ds(first * down_rows, count * down_rows), where
 
     def weight_x(w, q, kind):
         peer = lax.rem(tp + q, m)
@@ -303,8 +310,11 @@
             ring_meta(k + 2).start()
         for p in range(AG_PIECES):
             ring(k, p).wait_recv()
-            if k + 2 < n:
-                ring(k + 2, p).start()
+            onward = k + 2 if k + 2 < n - 1 or (k + 2 == n - 1 and p < AG_PIECES // 2) else None
+            if k == n - 2 and p >= AG_PIECES // 2:
+                onward = n - 1
+            if onward is not None:
+                ring(onward, p).start()
         for at in issue.get(k, ()):
             for kind in range(3):
                 weight_z(at, kind).start()
@@ -335,20 +345,27 @@
         for c in range(parts):
             rv_ref[g, c, pl.ds(lanes, own_h), :] = hd_ref[:, pl.ds(c * wide, wide)]
 
-    for w in range(groups):
-        if w not in moved_on:
-            move_on(w)
-    for w in range(groups):
+    def settle(w):
         for kind in range(3):
             weight_x_all(w, kind).wait_recv()
-        for at in range(w * GROUP, (w + 1) * GROUP):
+        for at in range(bundles[w][0], sum(bundles[w])):
             source = lax.rem(z + n + offset_of(order[at]), n)
             there = pl.ds(pl.multiple_of(source * deep, deep), deep)
-            gate_ref[:, there] = fg_ref[:, pl.ds(at * deep, deep)]
-            up_ref[:, there] = fu_ref[:, pl.ds(at * deep, deep)]
+            gate_ref[there, :] = jnp.transpose(fg_ref[:, pl.ds(at * deep, deep)])
+            up_ref[there, :] = jnp.transpose(fu_ref[:, pl.ds(at * deep, deep)])
             down_ref[pl.ds(pl.multiple_of(source * down_rows, down_rows), down_rows), :] = fd_ref[
                 pl.ds(at * down_rows, down_rows), :
             ]
+
+    settled = 0
+    for w in range(len(bundles)):
+        if w not in moved_on:
+            while settled < w - 1:
+                settle(settled)
+                settled += 1
+            move_on(w)
+    for w in range(settled, len(bundles)):
+        settle(w)
 
     for g in range(groups):
         exchange_all(g).wait_send()
@@ -358,14 +375,13 @@
         @pl.loop(0, count)
         def _(i):
             g = first - i
-            gate = jnp.zeros((lanes, gate_ref.shape[0]), jnp.float32)
-            upper = jnp.zeros((lanes, gate_ref.shape[0]), jnp.float32)
+            gate = jnp.zeros((lanes, gate_ref.shape[1]), jnp.float32)
+            upper = jnp.zeros((lanes, gate_ref.shape[1]), jnp.float32)
             for c in range(parts):
                 x = x_ref[g, c]
-                cols = pl.ds(c * wide, wide)
-                nt = (((1,), (1,)), ((), ()))
-                gate += lax.dot_general(x, gate_ref[:, cols], nt, preferred_element_type=jnp.float32)
-                upper += lax.dot_general(x, up_ref[:, cols], nt, preferred_element_type=jnp.float32)
+                deep_rows = pl.ds(c * wide, wide)
+                gate += jnp.dot(x, gate_ref[deep_rows, :], preferred_element_type=jnp.float32)
+                upper += jnp.dot(x, up_ref[deep_rows, :], preferred_element_type=jnp.float32)
             hidden = (gate / (1.0 + jnp.exp(-gate)) * upper).astype(jnp.bfloat16)
 
             @pl.loop(0, parts)
@@ -391,9 +407,11 @@
         return remote(mst_ref.at[r % 2, c], min_ref.at[r - 1, c],
                       m_send.at[r - 1, c], m_recv.at[r - 1, c], "fs", below)
 
-    def forward(sign, r, c):
-        last = half - 1 if sign > 0 else half
-        total = share(sign * r, c)
+    cut = (parts + 1) // 2
+
+    def forward(sign, r, c, low):
+        last = half if (sign < 0) == low else half - 1
+        total = share(sign * r if r < half else -half, c)
         if r < last:
             hop(sign, r + 1, c).wait_recv()
             total = total + (pin_ref if sign > 0 else min_ref)[r, c].astype(jnp.float32)
@@ -402,23 +420,43 @@
         (pst_ref if sign > 0 else mst_ref)[r % 2, c] = total.astype(jnp.bfloat16)
         hop(sign, r, c).start()
 
+    def steps(i, low):
+        if i == 0:
+            return ((-1, half), (1, half - 1)) if low else ((1, half), (-1, half - 1))
+        if i == 1 and not low:
+            return ((1, half - 1), (1, half - 2))
+        return (-1, half - i), (1, half - 1 - i)
+
     early = min(2, groups)
     experts(groups - 1, early)
     for i in range(half):
         g = groups - 1 - i // 2
-
-        @pl.loop(0, parts)
-        def _(c):
-            if i == 0:
-                combine(g, c)
-            forward(-1, half - i, c)
-            if half - 1 - i > 0:
-                forward(1, half - 1 - i, c)
-            if i % 2 == 1 and g > 0:
-                combine(g - 1, c)
-
-        if i == 0 and groups > early:
-            experts(groups - 1 - early, groups - early)
+        for low, first, end in ((True, 0, cut), (False, cut, parts)):
+            if first == end:
+                continue
+
+            @pl.loop(first, end)
+            def _(c):
+                if i == 0:
+                    combine(g, c)
+                for at, (sign, r) in enumerate(steps(i, low)):
+                    if r > 0 and not (at == 1 and i == 1 and not low):
+                        forward(sign, r, c, low)
+
+        for low, first, end in ((True, 0, cut), (False, cut, parts)):
+            late = i == 1 and not low and half > 2
+            if first == end or not (late or (i % 2 == 1 and g > 0)):
+                continue
+
+            @pl.loop(first, end)
+            def _(c):
+                if late:
+                    forward(*steps(i, low)[1], c, low)
+                if i % 2 == 1 and g > 0:
+                    combine(g - 1, c)
+
+        if i < groups - early:
+            experts(groups - 1 - early - i, 1)
 
     @pl.loop(0, parts)
     def _(c):
@@ -428,10 +466,9 @@
         out_ref[:, pl.ds(pl.multiple_of(c * wide, wide), wide)] = total.astype(jnp.bfloat16)
 
     for c in range(parts):
-        for r in range(1, min(2, half - 1) + 1):
-            hop(1, r, c).wait_send()
-        for r in range(1, min(2, half) + 1):
-            hop(-1, r, c).wait_send()
+        for sign in (-1, 1):
+            for r in range(1, min(2, half if (sign < 0) == (c < cut) else half - 1) + 1):
+                hop(sign, r, c).wait_send()
         for g in range(groups):
             answer_all(g, c).wait_send()
     for q in range(1, m):
@@ -443,10 +480,23 @@
         ring_meta(k).wait_send()
         for p in range(AG_PIECES):
             ring(k, p).wait_send()
-    for w in range(groups):
+    for w in range(len(bundles)):
         for kind in range(3):
             weight_z_all(w, kind).wait_send()
             weight_x_all(w, kind).wait_send()
+
+
+def hand_on(
+    mixed_ref, gate_ref, up_ref, down_ref, hgu_ref, hd_ref,
+    mixed_out, gate_out, up_out, down_out, shared_gate_out, shared_up_out, shared_down_out,
+):
+    mixed_out[...] = mixed_ref[...]
+    gate_out[0] = gate_ref[...]
+    up_out[0] = up_ref[...]
+    down_out[0] = down_ref[...]
+    shared_gate_out[...] = jnp.transpose(hgu_ref[0])
+    shared_up_out[...] = jnp.transpose(hgu_ref[1])
+    shared_down_out[...] = hd_ref[...]
 
 
 def on_device(
@@ -486,12 +536,12 @@
 
     place = jnp.asarray((lane % slots)[None, :].astype(np.float32))
     held = pl.BlockSpec(memory_space=pl.ANY)
-    mixed, gate_t, up_t, served_down, held_gu, held_down = pl.pallas_call(
+    results = pl.pallas_call(
         functools.partial(kernel, n, m, cap),
         out_shape=(
             jax.ShapeDtypeStruct((rows, width), bf16),
-            jax.ShapeDtypeStruct((hidden, width), bf16),
-            jax.ShapeDtypeStruct((hidden, width), bf16),
+            jax.ShapeDtypeStruct((width, hidden), bf16),
+            jax.ShapeDtypeStruct((width, hidden), bf16),
             jax.ShapeDtypeStruct((hidden, width), bf16),
             jax.ShapeDtypeStruct((2, hidden, deep), bf16),
             jax.ShapeDtypeStruct((down_rows, width), bf16),
@@ -523,15 +573,15 @@
             pltpu.VMEM((hidden, width), bf16),
             pltpu.VMEM((groups, GROUP * rows, lanes + own_h), bf16),
             pltpu.VMEM((parts, GROUP * rows, wide), f32),
-            pltpu.VMEM((half - 1, parts, rows, wide), bf16),
+            pltpu.VMEM((half, parts, rows, wide), bf16),
             pltpu.VMEM((half, parts, rows, wide), bf16),
             pltpu.VMEM((2, parts, rows, wide), bf16),
             pltpu.VMEM((2, parts, rows, wide), bf16),
             dma((n, AG_PIECES)), dma((n, AG_PIECES)), dma((n,)), dma((n,)),
             dma((groups,)), dma((groups,)), dma((groups, parts)), dma((groups, parts)),
             dma((m - 1,)), dma((m - 1,)), dma((m - 1,)), dma((m - 1,)), dma((n - 1,)), dma((n - 1,)),
-            dma((2, 3)), dma((groups, 3)), dma((groups, 3)), dma((groups, 3)), dma((groups, 3)),
-            dma((half - 1, parts)), dma((half - 1, parts)), dma((half, parts)), dma((half, parts)),
+            dma((2, 3)), *[dma((groups + 1, 3))] * 4,
+            *[dma((half, parts))] * 4,
         ],
         compiler_params=pltpu.CompilerParams(
             collective_id=0, has_side_effects=True, vmem_limit_bytes=63 * 1024 * 1024,
@@ -543,7 +593,19 @@
         turned(expert_gate), turned(expert_up), expert_down.reshape(n, m, down_rows, down_cols),
         expand(0), expand(m), place,
     )
-    return (mixed, gate_t.T[None], up_t.T[None], served_down[None], held_gu[0].T, held_gu[1].T, held_down)
+    whole = jax.ShapeDtypeStruct((1, width, hidden), bf16)
+    held_up = jax.ShapeDtypeStruct((deep, hidden), bf16)
+    return pl.pallas_call(
+        hand_on,
+        out_shape=(
+            jax.ShapeDtypeStruct((rows, width), bf16), whole, whole, jax.ShapeDtypeStruct((1, hidden, width), bf16),
+            held_up, held_up, jax.ShapeDtypeStruct((down_rows, width), bf16),
+        ),
+        in_specs=[VMEM] * 6,
+        out_specs=(VMEM,) * 7,
+        cost_estimate=pl.CostEstimate(flops=1_000_000, bytes_accessed=8_000_000, transcendentals=0),
+        name="hand_on",
+    )(*results)
 
 
 def solution(mesh):

time: 392 us -> 420 us (1.071)
  Pallas kernels: 384 us -> 420 us
  local copies, waits for them, and re-layouts: 7.59 us -> 0 us
    pallas_call x1, Pallas kernels: 384 us -> 416 us  [on_device(): pl.pallas_call(functools.partial(kernel, n, m, cap), out_shape=(jax.Shape...]
    unnamed x17 -> x0, local copies, waits for them, and re-layouts: 7.58 us -> none
where the time goes in v4:
time: 420 us
  Pallas kernels  420 us (100%)
    pallas_call x1, Pallas kernels, on_device(): pl.pallas_call(functools.partial(kernel, n, m, cap), out_shape=(jax.Shape...  416 us

profile of v4, /device:TPU:33, one launch (start us, length us, event | category | flops | bytes accessed | tf_op | source)
XLA Modules:
  0.0 420.3 jit_solution(1735893146600389377)
XLA Ops:
  0.6 415.6 %hand_over.1 = (bf16[128,2048]{1,0:T(8,128)(2,1)}, bf16[2048,256]{1,0:T(8,128)(2,1)}, bf16[2048,256]{1,0:T(8,128)(2,1)}, bf16[256,2048]{1,0:T(8,128)(2,1)}, bf16...) custom-call(bf16[128,2048]{1,0:T(8,128)(2,1)} %tok_ref.1, s32[8,128]{1,0:T(8,128)} %bitcast.17, f32[8,128]{1,0:T(8,128)} %bitcast.18, ...), custom_call_target="tpu_custom_call" | custom-call | flops 99999997952 | bytes 30000000 | tf_op jit(solution)/shard_map/hand_over/pallas_call | solution.py:539
  416.3 4.0 hand_on.1

commit v5 on v4

--- a/solution.py
+++ b/solution.py
@@ -303,7 +303,7 @@
 
     issue = {}
     for at in range(1, n):
-        issue.setdefault(max(1, min(n - 3, 1 + 2 * (at // 2))), []).append(at)
+        issue.setdefault(max(1, min(n - 2, 1 + 2 * (at // 2))), []).append(at)
     for k in range(1, n):
         ring_meta(k).wait_recv()
         if k + 2 < n:
@@ -407,11 +407,9 @@
         return remote(mst_ref.at[r % 2, c], min_ref.at[r - 1, c],
                       m_send.at[r - 1, c], m_recv.at[r - 1, c], "fs", below)
 
-    cut = (parts + 1) // 2
-
-    def forward(sign, r, c, low):
-        last = half if (sign < 0) == low else half - 1
-        total = share(sign * r if r < half else -half, c)
+    def forward(sign, r, c):
+        last = half - 1 if sign > 0 else half
+        total = share(sign * r, c)
         if r < last:
             hop(sign, r + 1, c).wait_recv()
             total = total + (pin_ref if sign > 0 else min_ref)[r, c].astype(jnp.float32)
@@ -420,40 +418,20 @@
         (pst_ref if sign > 0 else mst_ref)[r % 2, c] = total.astype(jnp.bfloat16)
         hop(sign, r, c).start()
 
-    def steps(i, low):
-        if i == 0:
-            return ((-1, half), (1, half - 1)) if low else ((1, half), (-1, half - 1))
-        if i == 1 and not low:
-            return ((1, half - 1), (1, half - 2))
-        return (-1, half - i), (1, half - 1 - i)
-
     early = min(2, groups)
     experts(groups - 1, early)
     for i in range(half):
         g = groups - 1 - i // 2
-        for low, first, end in ((True, 0, cut), (False, cut, parts)):
-            if first == end:
-                continue
-
-            @pl.loop(first, end)
-            def _(c):
-                if i == 0:
-                    combine(g, c)
-                for at, (sign, r) in enumerate(steps(i, low)):
-                    if r > 0 and not (at == 1 and i == 1 and not low):
-                        forward(sign, r, c, low)
-
-        for low, first, end in ((True, 0, cut), (False, cut, parts)):
-            late = i == 1 and not low and half > 2
-            if first == end or not (late or (i % 2 == 1 and g > 0)):
-                continue
-
-            @pl.loop(first, end)
-            def _(c):
-                if late:
-                    forward(*steps(i, low)[1], c, low)
-                if i % 2 == 1 and g > 0:
-                    combine(g - 1, c)
+
+        @pl.loop(0, parts)
+        def _(c):
+            if i == 0:
+                combine(g, c)
+            forward(-1, half - i, c)
+            if half - 1 - i > 0:
+                forward(1, half - 1 - i, c)
+            if i % 2 == 1 and g > 0:
+                combine(g - 1, c)
 
         if i < groups - early:
             experts(groups - 1 - early - i, 1)
@@ -466,9 +444,10 @@
         out_ref[:, pl.ds(pl.multiple_of(c * wide, wide), wide)] = total.astype(jnp.bfloat16)
 
     for c in range(parts):
-        for sign in (-1, 1):
-            for r in range(1, min(2, half if (sign < 0) == (c < cut) else half - 1) + 1):
-                hop(sign, r, c).wait_send()
+        for r in range(1, min(2, half - 1) + 1):
+            hop(1, r, c).wait_send()
+        for r in range(1, min(2, half) + 1):
+            hop(-1, r, c).wait_send()
         for g in range(groups):
             answer_all(g, c).wait_send()
     for q in range(1, m):

time: 420 us -> 403 us (0.960)
  Pallas kernels: 420 us -> 403 us
    pallas_call x1, Pallas kernels: 416 us -> 399 us  [on_device(): pl.pallas_call(functools.partial(kernel, n, m, cap), out_shape=(jax.Shape...]
where the time goes in v5:
time: 403 us
  Pallas kernels  403 us (100%)
    pallas_call x1, Pallas kernels, on_device(): pl.pallas_call(functools.partial(kernel, n, m, cap), out_shape=(jax.Shape...  399 us

profile of v5, /device:TPU:33, one launch (start us, length us, event | category | flops | bytes accessed | tf_op | source)
XLA Modules:
  0.0 403.2 jit_solution(9167578631273480976)
XLA Ops:
  0.6 398.6 %hand_over.1 = (bf16[128,2048]{1,0:T(8,128)(2,1)}, bf16[2048,256]{1,0:T(8,128)(2,1)}, bf16[2048,256]{1,0:T(8,128)(2,1)}, bf16[256,2048]{1,0:T(8,128)(2,1)}, bf16...) custom-call(bf16[128,2048]{1,0:T(8,128)(2,1)} %tok_ref.1, s32[8,128]{1,0:T(8,128)} %bitcast.17, f32[8,128]{1,0:T(8,128)} %bitcast.18, ...), custom_call_target="tpu_custom_call" | custom-call | flops 99999997952 | bytes 30000000 | tf_op jit(solution)/shard_map/hand_over/pallas_call | solution.py:518
  399.3 4.0 hand_on.1

commit v6 on v5

--- a/solution.py
+++ b/solution.py
@@ -48,11 +48,12 @@
 
 def weight_order(n):
     order, far, near = [0, n - 1], n - 2, 1
-    while near <= far:
-        order.append(far)
+    while near < far:
+        order += [far, far - 1]
+        far -= 2
         if near < far:
-            order.append(near)
-        far, near = far - 1, near + 1
+            order += [near, near + 1]
+            near += 2
     return order
 
 
@@ -104,13 +105,10 @@
 
     def ring(k, p):
         src = max(k - 2, 0)
-        upward = k % 2 == 1
-        if k == n - 1 and p >= AG_PIECES // 2:
-            src, upward = k - 1, False
         return remote(
             all_ref.at[pl.ds(src * rows + p * step_rows, step_rows), :],
             all_ref.at[pl.ds(k * rows + p * step_rows, step_rows), :],
-            ag_send.at[k, p], ag_recv.at[k, p], "fs", above if upward else below,
+            ag_send.at[k, p], ag_recv.at[k, p], "fs", above if k % 2 == 1 else below,
         )
 
     def ring_meta(k):
@@ -303,18 +301,15 @@
 
     issue = {}
     for at in range(1, n):
-        issue.setdefault(max(1, min(n - 2, 1 + 2 * (at // 2))), []).append(at)
+        issue.setdefault(max(1, min(n - 3, 1 + 2 * (at // 2))), []).append(at)
     for k in range(1, n):
         ring_meta(k).wait_recv()
         if k + 2 < n:
             ring_meta(k + 2).start()
         for p in range(AG_PIECES):
             ring(k, p).wait_recv()
-            onward = k + 2 if k + 2 < n - 1 or (k + 2 == n - 1 and p < AG_PIECES // 2) else None
-            if k == n - 2 and p >= AG_PIECES // 2:
-                onward = n - 1
-            if onward is not None:
-                ring(onward, p).start()
+            if k + 2 < n:
+                ring(k + 2, p).start()
         for at in issue.get(k, ()):
             for kind in range(3):
                 weight_z(at, kind).start()

time: 403 us -> 397 us (0.985)
  Pallas kernels: 403 us -> 396 us
    pallas_call x1, Pallas kernels: 399 us -> 392 us  [on_device(): pl.pallas_call(functools.partial(kernel, n, m, cap), out_shape=(jax.Shape...]
where the time goes in v6:
time: 397 us
  Pallas kernels  396 us (100%)
    pallas_call x1, Pallas kernels, on_device(): pl.pallas_call(functools.partial(kernel, n, m, cap), out_shape=(jax.Shape...  392 us

profile of v6, /device:TPU:33, one launch (start us, length us, event | category | flops | bytes accessed | tf_op | source)
XLA Modules:
  0.0 396.5 jit_solution(2821801262164890011)
XLA Ops:
  0.6 391.9 %hand_over.1 = (bf16[128,2048]{1,0:T(8,128)(2,1)}, bf16[2048,256]{1,0:T(8,128)(2,1)}, bf16[2048,256]{1,0:T(8,128)(2,1)}, bf16[256,2048]{1,0:T(8,128)(2,1)}, bf16...) custom-call(bf16[128,2048]{1,0:T(8,128)(2,1)} %tok_ref.1, s32[8,128]{1,0:T(8,128)} %bitcast.17, f32[8,128]{1,0:T(8,128)} %bitcast.18, ...), custom_call_target="tpu_custom_call" | custom-call | flops 99999997952 | bytes 30000000 | tf_op jit(solution)/shard_map/hand_over/pallas_call | solution.py:513
  392.6 4.0 %hand_on.1 = (bf16[128,2048]{1,0:T(8,128)(2,1)}, bf16[1,2048,256]{2,1,0:T(8,128)(2,1)}, bf16[1,2048,256]{2,1,0:T(8,128)(2,1)}, bf16[1,256,2048]{2,1,0:T(8,128)(2...) custom-call(bf16[128,2048]{1,0:T(8,128)(2,1)} %get-tuple-element.13.mixed_ref, ...), custom_call_target="tpu_custom_call" | custom-call | flops 1000000 | bytes 8000000 | tf_op jit(solution)/shard_map/hand_on/pallas_call | solution.py:572
